TPU v7x, 32 devices: a whole 2x2x4 slice. The times are simulated.
32 devices in a mesh: sp: 16 (over z, y, x), tp: 2 (over core).
Axes of the slice: x: 2, y: 2, z: 4, core: 2. Of those that a mesh axis runs over, the one named last changes fastest.
Arguments:
- residual_in: bfloat16 [8192, 2048], P(('sp', 'tp')), may hold values from -6 to 6
- queries: bfloat16 [8192, 2048], P('sp', 'tp'), may hold values from -200 to 200
- keys: bfloat16 [8192, 512], P('sp', 'tp'), may hold values from -5.5 to 5.5
- values: bfloat16 [8192, 512], P('sp', 'tp'), may hold values from -6 to 6
- docs: int32 [8192], P('sp'), may hold values from 0 to 3, never falling along the last dimension, each value on 1 to 4096 neighbouring positions
- sink: float32 [32], P('tp'), may hold values from 1 to 7
- out_weight: bfloat16 [2048, 2048], P('tp'), may hold values from -0.125 to 0.125
- gate_weight: bfloat16 [2048, 5632], P('sp', 'tp'), may hold values from -0.125 to 0.125
- up_weight: bfloat16 [2048, 5632], P('sp', 'tp'), may hold values from -0.125 to 0.125
- down_weight: bfloat16 [5632, 2048], P('tp', 'sp'), may hold values from -0.078125 to 0.078125
- conv_taps: float32 [3, 5632], P(None, 'tp'), may hold values from -3.5 to 3.5
- norm_gains: float32 [3, 2048], replicated, may hold values from 0.1 to 1.9
Outputs:
- layer_out: bfloat16 [8192, 2048], P(('sp', 'tp'))
All inputs are finite; a program needn't handle non-finite values.
Results may differ from a plain program's by a relative error of at most 0.02.
Values may be sent and summed in bfloat16 or wider, within the bound.
No kernel may reach another device: no remote copies, remote signals or barrier semaphores. Data moves between devices by JAX's collectives and lax.ppermute only.
A program may use at most 128 MiB of HBM per device.

v0:
```python
import jax
import jax.numpy as jnp
from jax import lax
from jax.sharding import PartitionSpec as P

HEAD = 64
WINDOW = 128


rope_base = 10000.0
neg_large = -1e30
norm_eps = 1e-06


def padded(cells, sides, width):
    for axis, dim in sides:
        count = lax.axis_size(axis)
        ends = count - 1
        head = lax.slice_in_dim(cells, 0, width, axis=dim)
        tail = lax.slice_in_dim(cells, cells.shape[dim] - width, cells.shape[dim], axis=dim)
        cells = jnp.concatenate(
            [
                lax.ppermute(tail, axis, [(i, (i + 1) % count) for i in range(ends)]),
                cells,
                lax.ppermute(head, axis, [((i + 1) % count, i) for i in range(ends)]),
            ],
            axis=dim,
        )
    return cells


def rotate(block, positions):
    rows = block.shape[0]
    heads = block.shape[1] // HEAD
    half = HEAD // 2
    freq = rope_base ** (-jnp.arange(half, dtype=jnp.float32) * 2.0 / HEAD)
    angle = positions.astype(jnp.float32)[:, None] * freq[None, :]
    cosine = jnp.cos(angle)[:, None, :]
    sine = jnp.sin(angle)[:, None, :]
    shaped = block.astype(jnp.float32).reshape(rows, heads, 2, half)
    first = shaped[:, :, 0]
    second = shaped[:, :, 1]
    turned = jnp.stack([first * cosine - second * sine, second * cosine + first * sine], axis=2)
    return turned.reshape(rows, heads * HEAD).astype(jnp.bfloat16)


def attend(queries, keys, values, allowed, sink):
    rows = queries.shape[0]
    kv_local = keys.shape[1] // HEAD
    group = queries.shape[1] // HEAD // kv_local
    shaped_q = queries.reshape(rows, kv_local, group, HEAD)
    shaped_k = keys.reshape(keys.shape[0], kv_local, HEAD)
    shaped_v = values.reshape(values.shape[0], kv_local, HEAD)
    scores = jnp.einsum(
        "qngd,knd->ngqk", shaped_q, shaped_k, preferred_element_type=jnp.float32
    ) * HEAD ** (-0.5)
    scores = jnp.where(allowed[None, None], scores, neg_large)
    sink_group = sink.reshape(kv_local, group)[:, :, None]
    top = jnp.maximum(jnp.max(scores, axis=-1), sink_group)
    weights = jnp.exp(scores - top[..., None])
    total = jnp.sum(weights, axis=-1) + jnp.exp(sink_group - top)
    probs = (weights / total[..., None]).astype(jnp.bfloat16)
    out = jnp.einsum("ngqk,knd->qngd", probs, shaped_v, preferred_element_type=jnp.float32)
    return out.reshape(rows, kv_local * group * HEAD).astype(jnp.bfloat16)


def normalize(vector, gain):
    scale = lax.rsqrt(jnp.mean(vector * vector, axis=-1, keepdims=True) + norm_eps)
    return vector * scale * gain


def local(
    residual_in,
    queries,
    keys,
    values,
    docs,
    sink,
    out_weight,
    gate_weight,
    up_weight,
    down_weight,
    conv_taps,
    norm_gains,
):
    rows = queries.shape[0]
    offset = lax.axis_index("sp") * rows
    total_len = lax.axis_size("sp") * rows
    keys_ext, values_ext, docs_ext = (
        padded(keys, (("sp", 0),), WINDOW),
        padded(values, (("sp", 0),), WINDOW),
        padded(docs, (("sp", 0),), WINDOW),
    )
    here = offset + jnp.arange(rows, dtype=jnp.int32)
    there = offset - WINDOW + jnp.arange(rows + 2 * WINDOW, dtype=jnp.int32)
    q_rot = rotate(queries, here)
    k_rot = rotate(keys_ext, there)
    allowed = (
        (jnp.abs(there[None, :] - here[:, None]) <= WINDOW)
        & (there[None, :] >= 0)
        & (there[None, :] < total_len)
        & (docs_ext[None, :] == docs[:, None])
    )
    attended = attend(q_rot, k_rot, values_ext, allowed, sink)
    mixed = lax.psum_scatter(
        jnp.dot(attended, out_weight, preferred_element_type=jnp.float32).astype(jnp.bfloat16),
        "tp",
        scatter_dimension=0,
        tiled=True,
    ).astype(jnp.float32)
    updated = (residual_in.astype(jnp.float32) + normalize(mixed, norm_gains[0])).astype(
        jnp.bfloat16
    )
    normed = normalize(updated.astype(jnp.float32), norm_gains[1]).astype(jnp.bfloat16)
    ffn_in = lax.all_gather(normed, "tp", axis=0, tiled=True)
    gate = jnp.dot(
        ffn_in,
        lax.all_gather(gate_weight, "sp", axis=0, tiled=True),
        preferred_element_type=jnp.float32,
    )
    up = jnp.dot(
        ffn_in,
        lax.all_gather(up_weight, "sp", axis=0, tiled=True),
        preferred_element_type=jnp.float32,
    )
    gate_low = gate.astype(jnp.bfloat16)
    gate_ext = padded(gate_low, (("sp", 0),), 1).astype(jnp.float32)
    same_prev = (docs_ext[WINDOW - 1 : WINDOW - 1 + rows] == docs)[:, None]
    same_next = (docs_ext[WINDOW + 1 : WINDOW + 1 + rows] == docs)[:, None]
    conv = (
        conv_taps[0] * jnp.where(same_prev, gate_ext[:-2], 0.0)
        + conv_taps[1] * gate_ext[1:-1]
        + conv_taps[2] * jnp.where(same_next, gate_ext[2:], 0.0)
    )
    hidden = (jax.nn.silu(conv) * up).astype(jnp.bfloat16)
    terms = jnp.dot(
        hidden,
        lax.all_gather(down_weight, "sp", axis=1, tiled=True),
        preferred_element_type=jnp.float32,
    )
    ffn_out = lax.psum_scatter(
        terms.astype(jnp.bfloat16), "tp", scatter_dimension=0, tiled=True
    ).astype(jnp.float32)
    return (updated.astype(jnp.float32) + normalize(ffn_out, norm_gains[2])).astype(jnp.bfloat16)


def solution(mesh):
    in_specs = (
        P(("sp", "tp"), None),
        P("sp", "tp"),
        P("sp", "tp"),
        P("sp", "tp"),
        P("sp"),
        P("tp"),
        P("tp", None),
        P("sp", "tp"),
        P("sp", "tp"),
        P("tp", "sp"),
        P(None, "tp"),
        P(),
    )
    out_specs = P(("sp", "tp"), None)
    return jax.shard_map(local, mesh=mesh, in_specs=in_specs, out_specs=out_specs, check_vma=False)
```

profile of v0, /device:TPU:0, one launch (start us, length us, event | category | flops | bytes accessed | tf_op | source)
XLA Modules:
  0.0 611.7 jit_solution(4927613826209139854)
XLA Ops:
  7.7 4.9 collective-permute-start.4
  14.6 4.5 collective-permute-start.2
  20.5 1.5 fusion.36
  22.0 4.9 collective-permute-start
  34.4 5.1 fusion.1
  39.6 5.3 fusion
  44.9 3.0 copy-done
  48.8 12.0 %fusion.24 = bf16[4,64,4,512]{3,1,2,0:T(8,128)(2,1)S(1)} fusion(bf16[768,4,64,1]{0,2,3,1:T(8,128)(2,1)S(1)} %bitcast.47, f32[4,768,512,4]{2,1,3,0:T(8,128)} %copy-done, f32[4,4,512]{2,1,0:T(4,128)} %exponential_add_fusion, f32[4,4,512]{2,1,0:T(4,128)S(1)} %broadcast_maximum_fusion, pred[512,768]{0,1:T(8,128)(4,1)S(1)} %fusion.23), kind=kOutput, calls=%fused_computation.42 | convolution fusion | flops 837287936 | bytes 27066368 | tf_op jit(solution)/shard_map/ngqk,knd->qngd/dot_general | solution.py:63
  60.9 3.8 convolution_convert_fusion.1
  64.8 15.3 %reduce-scatter.3.cloned.1.call-done = bf16[256,2048]{1,0:T(8,128)(2,1)} async-done(((bf16[512,2048]{1,0:T(8,128)(2,1)}), bf16[256,2048]{1,0:T(8,128)(2,1)}) %reduce-scatter.3.cloned.1.call-update) | async-done | bytes 1048592 | tf_op jit(solution)/shard_map/reduce_scatter | solution.py:105
  80.1 1.5 fusion.11
  81.7 1.9 fusion.17
  87.1 9.8 %all-gather.5.cloned.1.call-done = bf16[512,2048]{1,0:T(8,128)(2,1)} async-done(((bf16[256,2048]{1,0:T(8,128)(2,1)}), bf16[512,2048]{1,0:T(8,128)(2,1)}) %all-gather.5.cloned.1.call-update) | async-done | bytes 2097168 | tf_op jit(solution)/shard_map/all_gather | solution.py:115
  96.9 145.4 %all-gather.7.cloned.1.call-done = bf16[2048,2816]{1,0:T(8,128)(2,1)} async-done(((bf16[128,2816]{1,0:T(8,128)(2,1)}), bf16[2048,2816]{1,0:T(8,128)(2,1)}) %all-gather.7.cloned.1.call-update) | async-done | bytes 11534352 | tf_op jit(solution)/shard_map/all_gather | solution.py:118
  242.3 10.9 %convolution_convert_fusion = bf16[512,2816]{1,0:T(8,128)(2,1)S(1)} fusion(bf16[512,2048]{1,0:T(8,128)(2,1)} %all-gather.5.cloned.1.call-done, bf16[2048,2816]{1,0:T(8,128)(2,1)} %all-gather.7.cloned.1.call-done), kind=kOutput, calls=%fused_computation.14 | convolution fusion | flops 5907021824 | bytes 16515072 | tf_op jit(solution)/shard_map/dot_general | solution.py:116
  253.3 3.2 collective-permute-start.6
  258.0 4.4 collective-permute-done.7
  262.4 3.1 maximum_convert_fusion
  265.5 159.9 %all-gather.11.cloned.1.call-done = bf16[2816,2048]{1,0:T(8,128)(2,1)} async-done(((bf16[2816,128]{1,0:T(8,128)(2,1)}), bf16[2816,2048]{1,0:T(8,128)(2,1)}) %all-gather.11.cloned.1.call-update) | async-done | bytes 11534352 | tf_op jit(solution)/shard_map/all_gather | solution.py:138
  425.3 142.2 %all-gather.9.cloned.1.call-done = bf16[2048,2816]{1,0:T(8,128)(2,1)} async-done(((bf16[128,2816]{1,0:T(8,128)(2,1)}), bf16[2048,2816]{1,0:T(8,128)(2,1)}) %all-gather.9.cloned.1.call-update) | async-done | bytes 11534352 | tf_op jit(solution)/shard_map/all_gather | solution.py:123
  567.6 25.0 %convolution_convert_fusion.2 = bf16[512,2048]{1,0:T(8,128)(2,1)} fusion(bf16[2816,2048]{1,0:T(8,128)(2,1)} %all-gather.11.cloned.1.call-done, f32[514,2816]{1,0:T(8,128)} %maximum_convert_fusion, f32[2816]{0:T(1024)S(1)} %get-tuple-element.6, f32[2816]{0:T(1024)S(1)} %get-tuple-element.7, f32[2816]{0:T(1024)S(1)} %get-tuple-element.5, ...), kind=kOutput, calls=%fused_computation.19 | convolution fusion | flops 11830951936 | bytes 44599296 | tf_op jit(solution)/shard_map/dot_general | solution.py:136
  592.6 8.1 %reduce-scatter.5.cloned.1.call-done = bf16[256,2048]{1,0:T(8,128)(2,1)} async-done(((bf16[512,2048]{1,0:T(8,128)(2,1)}), bf16[256,2048]{1,0:T(8,128)(2,1)}) %reduce-scatter.5.cloned.1.call-update) | async-done | bytes 1048592 | tf_op jit(solution)/shard_map/reduce_scatter | solution.py:141
  600.7 1.5 fusion.15
  602.2 2.6 fusion.20
  (72 shorter events, 17.9 us)
Async XLA Ops:
  6.5 73.6 %reduce-scatter.3.cloned.1.call-start = ((), (), s32[]{:S(2)}) async-start(), calls=%async_computation.2 | async-start | bytes 3145728 | tf_op jit(solution)/shard_map/reduce_scatter | solution.py:105
  7.6 23.3 %copy-start.6 = (f32[16]{0:T(128)S(1)}, f32[16]{0:T(128)}, u32[]{:S(2)}) copy-start(f32[16]{0:T(128)} %param.17) | copy-start | bytes 196
  7.6 24.7 %copy-start.3 = (s32[512]{0:T(512)S(1)}, s32[512]{0:T(512)}, u32[]{:S(2)}) copy-start(s32[512]{0:T(512)} %param.16) | copy-start | bytes 6148
  7.7 25.7 %collective-permute-start.4 = (bf16[128,256]{0,1:T(8,128)(2,1)S(1)}, bf16[128,256]{0,1:T(8,128)(2,1)S(1)}, u32[]{:S(2)}, u32[]{:S(2)}) collective-permute-start(bf16[128,256]{0,1:T(8,128)(2,1)S(1)} %get-tuple-element.16), channel_id=1, source_target_pairs={{0,2},{2,4},{4,6},{6,8},{8,10},{10,12},{12,14},{14,16},{16,18},{18... | collective-permute-start | bytes 196616 | tf_op jit(solution)/shard_map/ppermute | solution.py:23
  12.6 20.9 %collective-permute-start.5 = (bf16[128,256]{0,1:T(8,128)(2,1)S(1)}, bf16[128,256]{0,1:T(8,128)(2,1)S(1)}, u32[]{:S(2)}, u32[]{:S(2)}) collective-permute-start(bf16[128,256]{0,1:T(8,128)(2,1)S(1)} %get-tuple-element.17), channel_id=1, source_target_pairs={{2,0},{4,2},{6,4},{8,6},{10,8},{12,10},{14,12},{16,14},{18,16},{20... | collective-permute-start | bytes 196616 | tf_op jit(solution)/shard_map/ppermute | solution.py:25
  14.6 16.4 %collective-permute-start.2 = (s32[128]{0:T(128)S(1)}, s32[128]{0:T(128)S(1)}, u32[]{:S(2)}, u32[]{:S(2)}) collective-permute-start(s32[128]{0:T(128)S(1)} %get-tuple-element.31), channel_id=1, source_target_pairs={{0,2},{2,4},{4,6},{6,8},{8,10},{10,12},{12,14},{14,16},{16,18},{18... | collective-permute-start | bytes 1544 | tf_op jit(solution)/shard_map/ppermute | solution.py:23
  19.2 13.2 %collective-permute-start.3 = (s32[128]{0:T(128)S(1)}, s32[128]{0:T(128)S(1)}, u32[]{:S(2)}, u32[]{:S(2)}) collective-permute-start(s32[128]{0:T(128)S(1)} %get-tuple-element.32), channel_id=1, source_target_pairs={{2,0},{4,2},{6,4},{8,6},{10,8},{12,10},{14,12},{16,14},{18,16},{20... | collective-permute-start | bytes 1544 | tf_op jit(solution)/shard_map/ppermute | solution.py:25
  22.0 26.6 %collective-permute-start = (bf16[128,256]{1,0:T(8,128)(2,1)}, bf16[128,256]{1,0:T(8,128)(2,1)S(1)}, u32[]{:S(2)}, u32[]{:S(2)}) collective-permute-start(bf16[128,256]{1,0:T(8,128)(2,1)} %get-tuple-element.18), channel_id=1, source_target_pairs={{0,2},{2,4},{4,6},{6,8},{8,10},{10,12},{12,14},{14,16},{16,18},{18... | collective-permute-start | bytes 196616 | tf_op jit(solution)/shard_map/ppermute | solution.py:23
  31.0 17.6 %collective-permute-start.1 = (bf16[128,256]{1,0:T(8,128)(2,1)}, bf16[128,256]{1,0:T(8,128)(2,1)S(1)}, u32[]{:S(2)}, u32[]{:S(2)}) collective-permute-start(bf16[128,256]{1,0:T(8,128)(2,1)} %get-tuple-element.19), channel_id=1, source_target_pairs={{2,0},{4,2},{6,4},{8,6},{10,8},{12,10},{14,12},{16,14},{18,16},{20... | collective-permute-start | bytes 196616 | tf_op jit(solution)/shard_map/ppermute | solution.py:25
  39.5 8.4 %copy-start = (f32[4,768,512,4]{2,1,3,0:T(8,128)}, f32[4,768,512,4]{2,1,3,0:T(8,128)S(1)}, u32[]{:S(2)}) copy-start(f32[4,768,512,4]{2,1,3,0:T(8,128)S(1)} %get-tuple-element.34) | copy-start | bytes 75497472
  39.6 9.0 %copy-start.2 = (bf16[512,256]{1,0:T(8,128)(2,1)S(1)}, bf16[512,256]{1,0:T(8,128)(2,1)}, u32[]{:S(2)}) copy-start(bf16[512,256]{1,0:T(8,128)(2,1)} %param.15) | copy-start | bytes 786436
  48.8 12.0 %copy-start.7 = (bf16[1024,2048]{1,0:T(8,128)(2,1)S(1)}, bf16[1024,2048]{1,0:T(8,128)(2,1)}, u32[]{:S(2)}) copy-start(bf16[1024,2048]{1,0:T(8,128)(2,1)} %param.18) | copy-start | bytes 12582916
  60.9 3.9 copy-start.5
  60.9 20.8 %copy-start.1 = (bf16[256,2048]{1,0:T(8,128)(2,1)S(1)}, bf16[256,2048]{1,0:T(8,128)(2,1)}, u32[]{:S(2)}) copy-start(bf16[256,2048]{1,0:T(8,128)(2,1)} %param.12) | copy-start | bytes 3145732
  64.7 22.3 %copy-start.4 = (f32[3,2816]{1,0:T(4,128)S(1)}, f32[3,2816]{1,0:T(4,128)}, u32[]{:S(2)}) copy-start(f32[3,2816]{1,0:T(4,128)} %param.22) | copy-start | bytes 101380
  64.7 32.2 %all-gather.5.cloned.1.call-start = ((), (), s32[]{:S(2)}) async-start(), calls=%async_computation.3 | async-start | bytes 3145728 | tf_op jit(solution)/shard_map/all_gather | solution.py:115
  84.9 157.4 %all-gather.7.cloned.1.call-start = ((), (), s32[]{:S(2)}) async-start(), calls=%async_computation.4 | async-start | bytes 12255232 | tf_op jit(solution)/shard_map/all_gather | solution.py:118
  85.6 339.7 %all-gather.11.cloned.1.call-start = ((), (), s32[]{:S(2)}) async-start(), calls=%async_computation.6 | async-start | bytes 12255232 | tf_op jit(solution)/shard_map/all_gather | solution.py:138
  86.2 481.4 %all-gather.9.cloned.1.call-start = ((), (), s32[]{:S(2)}) async-start(), calls=%async_computation.5 | async-start | bytes 12255232 | tf_op jit(solution)/shard_map/all_gather | solution.py:123
  86.8 513.9 %reduce-scatter.5.cloned.1.call-start = ((), (), s32[]{:S(2)}) async-start(), calls=%async_computation.7 | async-start | bytes 3145728 | tf_op jit(solution)/shard_map/reduce_scatter | solution.py:141
  253.3 4.7 collective-permute-start.6
  256.4 5.9 collective-permute-start.7
Sparse Core Ops, SparseCore 0:
  64.8 15.2 reduce-scatter.2
  85.0 11.8 all-gather.4
  99.7 142.5 all-gather.6
  244.8 180.4 all-gather.10
  427.9 139.5 all-gather.8
  592.7 7.9 reduce-scatter.4
where the time goes:
time: 612 us
  waiting for transfers between devices  487 us (80%)
  matrix products  56.8 us (9%)
  starting transfers between devices  23 us (4%)
  other arithmetic  22.6 us (4%)
  between operations  13.9 us (2%)
  local copies, waits for them, and re-layouts  8.33 us (1%)
    all_gather x1, waiting for transfers between devices, local(): lax.all_gather(down_weight, 'sp', axis=1, tiled=True)  160 us
    all_gather x1, waiting for transfers between devices, local(): lax.all_gather(gate_weight, 'sp', axis=0, tiled=True)  145 us
    all_gather x1, waiting for transfers between devices, local(): lax.all_gather(up_weight, 'sp', axis=0, tiled=True)  142 us
    dot_general x1, matrix products, local(): jnp.dot(hidden, lax.all_gather(down_weight, 'sp', axis=1, tiled=True), pr...  25 us
    ppermute x4, starting transfers between devices, padded(): lax.ppermute(tail, axis, [(i, (i + 1) % count) for i in range(ends)])  17.5 us
    reduce_scatter x1, waiting for transfers between devices, local(): lax.psum_scatter(jnp.dot(attended, out_weight, preferred_element_type=jnp...  15.3 us
  transfers between devices with their start and end apart: 14, of which 8 were waited for; matrix products, arithmetic and copies ran while one was open for 6% of the time, Pallas kernels for 0%

commit v1 on v0

--- a/solution.py
+++ b/solution.py
@@ -1,7 +1,10 @@
 import jax
 import jax.numpy as jnp
 from jax import lax
+from jax.experimental import pallas as pl
+from jax.experimental.pallas import tpu as pltpu
 from jax.sharding import PartitionSpec as P
+
 
 HEAD = 64
 WINDOW = 128
@@ -69,7 +72,7 @@
     return vector * scale * gain
 
 
-def local(
+def plain(
     residual_in,
     queries,
     keys,
@@ -144,6 +147,569 @@
     return (updated.astype(jnp.float32) + normalize(ffn_out, norm_gains[2])).astype(jnp.bfloat16)
 
 
+LANES = 128
+X, Y, ZL, FAR = 1, 2, 4, 8
+low = jnp.bfloat16
+full = jnp.float32
+params = pltpu.CompilerParams(vmem_limit_bytes=60 * 1024 * 1024)
+
+
+def hbm():
+    return pl.BlockSpec(memory_space=pl.ANY)
+
+
+def vmem():
+    return pl.BlockSpec(memory_space=pltpu.VMEM)
+
+
+def smem():
+    return pl.BlockSpec(memory_space=pltpu.SMEM)
+
+
+def cost(flops, bytes_accessed):
+    return pl.CostEstimate(flops=flops, bytes_accessed=bytes_accessed, transcendentals=0)
+
+
+def swap(cells, bit):
+    return lax.ppermute(cells, "sp", [(i, i ^ bit) for i in range(lax.axis_size("sp"))])
+
+
+def pick(cells, index, axis):
+    return lax.dynamic_index_in_dim(cells, index, axis, keepdims=False)
+
+
+class Place:
+    def __init__(self):
+        self.me = lax.axis_index("sp")
+        self.core = lax.axis_index("tp")
+        self.count = lax.axis_size("sp")
+        self.cores = lax.axis_size("tp")
+        self.x = self.me & 1
+        self.y = (self.me >> 1) & 1
+        self.zl = (self.me >> 2) & 1
+        self.fars = self.count // FAR
+
+    def other_core(self, cells):
+        return lax.ppermute(cells, "tp", [(i, i ^ 1) for i in range(self.cores)])
+
+    def far_shift(self, cells, step):
+        hops = [(i, (i + step * FAR) % self.count) for i in range(self.count)]
+        return lax.ppermute(cells, "sp", hops)
+
+
+def exchange(at, parts):
+    kept = pick(parts, at.x, 1)
+    came = swap(pick(parts, 1 - at.x, 1), X)
+    sent = jnp.stack([pick(kept, 1 - at.zl, 0), pick(came, 1 - at.zl, 0)])
+    mine = jnp.stack([pick(kept, at.zl, 0), pick(came, at.zl, 0)])
+    return jnp.concatenate([mine, swap(sent, ZL)])
+
+
+def spread(at, parts):
+    four = exchange(at, parts)
+    pieces = [(0, 0, four), (0, 1, swap(four, Y))]
+    for step in range(1, at.fars):
+        away = at.far_shift(four, step)
+        pieces += [(step, 0, away), (step, 1, swap(away, Y))]
+    return pieces
+
+
+OFFSETS = (0, X, ZL, X | ZL)
+
+
+def shard_of(me, fars, step, y, slot):
+    near = (me & 7) ^ (OFFSETS[slot] | (Y if y else 0))
+    return near + FAR * lax.rem((me >> 3) - step + fars, fars)
+
+
+def load_rows(me, spots, refs, whole, sems, depth, fars):
+    copies = []
+    for (step, y), ref in zip(spots, refs):
+        for slot in range(4):
+            shard = shard_of(me, fars, step, y, slot)
+            rows = pl.ds(pl.multiple_of(shard * depth, depth), depth)
+            copies.append(
+                pltpu.make_async_copy(ref.at[slot], whole.at[rows], sems.at[len(copies)])
+            )
+    for copy in copies:
+        copy.start()
+    return copies
+
+
+def attend_body(half_ref, sink_ref, q_ref, near_ref, cos_ref, sin_ref, weight_ref, out_ref, kd, vd, held):
+    kv = held.shape[1] // 4
+    span = kd.shape[1]
+    rows = held.shape[0]
+    step = WINDOW
+    window = 3 * step
+    start = pl.multiple_of(half_ref[0] * rows, rows)
+    lane = lax.broadcasted_iota(jnp.int32, (1, LANES), 1)
+    front = lane % HEAD < HEAD // 2
+    left = lane < HEAD
+
+    def rotated(cells, cosine, sine):
+        partner = jnp.where(
+            front, pltpu.roll(cells, LANES - HEAD // 2, 1), pltpu.roll(cells, HEAD // 2, 1)
+        )
+        return (cells * cosine + partner * sine).astype(low)
+
+    def doubled(cells, store, t):
+        turned = pltpu.roll(cells, HEAD, 1)
+        store[2 * t] = jnp.where(left, cells, turned).astype(low)
+        store[2 * t + 1] = jnp.where(left, turned, cells).astype(low)
+
+    reach = pl.ds(start, span)
+    for t in range(kv // LANES):
+        cells = near_ref[reach, t * LANES : (t + 1) * LANES].astype(full)
+        cells = rotated(cells, cos_ref[reach, :], sin_ref[reach, :]).astype(full)
+        doubled(cells, kd, t)
+        columns = slice(kv + t * LANES, kv + (t + 1) * LANES)
+        doubled(near_ref[reach, columns].astype(full), vd, t)
+
+    tags = near_ref[reach, 2 * kv :].astype(full)
+    across = jnp.concatenate(
+        [jnp.transpose(tags[i : i + step])[0:1] for i in range(0, span, step)], axis=1
+    )
+    gap = lax.broadcasted_iota(jnp.int32, (step, window), 1) - lax.broadcasted_iota(
+        jnp.int32, (step, window), 0
+    )
+    band = (gap >= 0) & (gap <= 2 * step)
+    for j in range(rows // step):
+        mine = tags[step + j * step : 2 * step + j * step, 0:1]
+        theirs = across[:, j * step : j * step + window]
+        bias = jnp.where(band & (mine == theirs), 0.0, neg_large)
+        at_rows = pl.ds(pl.multiple_of(start + j * step, step), step)
+        mid_rows = pl.ds(pl.multiple_of(start + (j + 1) * step, step), step)
+        cosine = cos_ref[mid_rows, :] * HEAD ** (-0.5)
+        sine = sin_ref[mid_rows, :] * HEAD ** (-0.5)
+
+        def one(n, carry):
+            stack = []
+            for t in range(2):
+                columns = pl.ds(pl.multiple_of((2 * n + t) * LANES, LANES), LANES)
+                cells = rotated(q_ref[at_rows, columns].astype(full), cosine, sine)
+                none = jnp.zeros_like(cells)
+                stack += [jnp.where(left, cells, none), jnp.where(left, none, cells)]
+            keys = kd[n, j * step : j * step + window]
+            scores = lax.dot_general(
+                jnp.concatenate(stack, axis=0),
+                keys,
+                (((1,), (1,)), ((), ())),
+                preferred_element_type=full,
+            )
+            probs = []
+            shares = []
+            for h in range(4):
+                part = scores[h * step : (h + 1) * step] + bias
+                sink = sink_ref[4 * n + h]
+                top = jnp.maximum(jnp.max(part, axis=1, keepdims=True), sink)
+                weights = jnp.exp(part - top)
+                total = jnp.sum(weights, axis=1, keepdims=True) + jnp.exp(sink - top)
+                probs.append(weights.astype(low))
+                shares.append(1.0 / total)
+            seen = jnp.dot(
+                jnp.concatenate(probs, axis=0),
+                vd[n, j * step : j * step + window],
+                preferred_element_type=full,
+            )
+            parts = [seen[h * step : (h + 1) * step] * shares[h] for h in range(4)]
+            for t in range(2):
+                columns = pl.ds(pl.multiple_of((2 * n + t) * LANES, LANES), LANES)
+                held[j * step : (j + 1) * step, columns] = jnp.where(
+                    left, parts[2 * t], parts[2 * t + 1]
+                ).astype(low)
+            return carry
+
+        lax.fori_loop(0, kv // HEAD, one, 0)
+    out_ref[...] = jnp.dot(held[...], weight_ref[...], preferred_element_type=full).astype(low)
+
+
+def normalize_body(core_ref, residual_ref, own_ref, given_ref, gains_ref, near_ref, updated_ref, packed_ref):
+    rows, width = residual_ref.shape
+    mixed = own_ref[...].astype(full) + given_ref[...].astype(full)
+    updated = residual_ref[...].astype(full) + normalize(mixed, gains_ref[0:1])
+    updated = updated.astype(low)
+    updated_ref[...] = updated
+    packed_ref[:, :width] = normalize(updated.astype(full), gains_ref[1:2]).astype(low)
+    edge = 16
+    start = pl.multiple_of(WINDOW - edge + core_ref[0] * rows, edge)
+    tags = near_ref[pl.ds(start, rows + 2 * edge), near_ref.shape[1] - LANES :].astype(full)
+    size = rows + 2 * edge
+    before = pltpu.roll(tags, 1, 0)
+    after = pltpu.roll(tags, size - 1, 0)
+    code = jnp.where(before == tags, 1.0, 0.0) + jnp.where(after == tags, 2.0, 0.0)
+    packed_ref[:, width:] = code[edge : edge + rows].astype(low)
+
+
+def product_body(spots, fars, count, width, me_ref, *refs):
+    tokens, pieces = refs[:count], refs[count : count + len(spots)]
+    gate_ref, up_ref, whole, held, weight_sems, token_sems = refs[count + len(spots) :]
+    depth = pieces[0].shape[1]
+    each, rows, cells = gate_ref.shape
+    at = pl.program_id(0)
+
+    @pl.when(at == 0)
+    def _():
+        copies = load_rows(me_ref[0], spots, pieces, whole, weight_sems, depth, fars)
+        for b in range(count):
+            block = held.at[b * rows : (b + 1) * rows]
+            pltpu.make_async_copy(tokens[b].at[:, :width], block, token_sems.at[b]).start()
+        for copy in copies:
+            copy.wait()
+
+    for b in range(each):
+        block = held.at[pl.ds(0, rows)]
+        pltpu.make_async_copy(block, block, token_sems.at[at * each + b]).wait()
+    start = pl.multiple_of(at * each * rows, each * rows)
+    both = jnp.dot(held[pl.ds(start, each * rows)], whole[...], preferred_element_type=full)
+    both = both.reshape(each, rows, 2 * cells)
+    gate_ref[...] = both[:, :, :cells].astype(low)
+    up_ref[...] = both[:, :, cells:]
+
+
+def hidden_body(gate_ref, up_ref, code_ref, around_ref, taps_ref, own_ref, other_ref):
+    each, _, rows, cells = gate_ref.shape
+    for b in range(each):
+        out_ref = (own_ref, other_ref)[b]
+        code = code_ref[b, 0].astype(full)
+        same_prev = (code == 1.0) | (code == 3.0)
+        same_next = code >= 2.0
+        index = lax.broadcasted_iota(jnp.int32, code.shape, 0)
+        for start in range(0, cells, LANES):
+            size = min(LANES, cells - start)
+            columns = slice(start, start + size)
+            gate = gate_ref[b, 0, :, columns].astype(full)
+            top, bottom = around_ref[b, 0, 0:1, columns], around_ref[b, 0, 1:2, columns]
+            at = index[:, :size]
+            before = jnp.where(at == 0, top.astype(full), pltpu.roll(gate, 1, 0))
+            after = jnp.where(at == rows - 1, bottom.astype(full), pltpu.roll(gate, rows - 1, 0))
+            conv = (
+                taps_ref[0:1, columns] * jnp.where(same_prev[:, :size], before, 0.0)
+                + taps_ref[1:2, columns] * gate
+                + taps_ref[2:3, columns] * jnp.where(same_next[:, :size], after, 0.0)
+            )
+            share = 0.5 * jnp.tanh(0.5 * conv) + 0.5
+            out_ref[0, :, columns] = (conv * share * up_ref[b, 0, :, columns]).astype(low)
+
+
+def down_body(spots, me_ref, *refs):
+    total = 2 * len(spots)
+    pieces, hiddens = refs[:total], refs[total : total + 8]
+    out_refs = refs[total + 8 : total + 10]
+    whole, sems = refs[total + 10 :]
+    cells = pieces[0].shape[2]
+    groups = len(out_refs)
+    each = len(spots) // groups
+    copies = [[] for _ in range(groups)]
+    for half in range(2):
+        for p in range(len(spots)):
+            for slot in range(4):
+                near = me_ref[0] ^ OFFSETS[slot]
+                place = (p % each) * 4 + (near & 1) + 2 * ((near >> 2) & 1)
+                columns = pl.ds(pl.multiple_of(place * cells, cells), cells)
+                index = (half * len(spots) + p) * 4 + slot
+                copies[p // each].append(
+                    pltpu.make_async_copy(
+                        pieces[half * len(spots) + p].at[slot],
+                        whole.at[p // each, half, :, columns],
+                        sems.at[index],
+                    )
+                )
+    for group in copies:
+        for copy in group:
+            copy.start()
+    for g, out_ref in enumerate(out_refs):
+        for copy in copies[g]:
+            copy.wait()
+        picked = spots[g]
+        size = cells * 4 * each // 2
+
+        def step(i, carry):
+            columns = pl.ds(pl.multiple_of(i * size, size), size)
+            sums = 0.0
+            for half in range(2):
+                rows = []
+                for b in picked:
+                    first = 4 * half + 2 * (b & 1)
+                    parts = [hiddens[first + c][b >> 1] for c in (0, 1)]
+                    rows.append(jnp.concatenate(parts, axis=1))
+                sums = sums + jnp.dot(
+                    jnp.concatenate(rows, axis=0),
+                    whole[g, half, :, columns],
+                    preferred_element_type=full,
+                )
+            out_ref[:, :, columns] = sums.astype(low).reshape(len(picked), -1, size)
+            return carry
+
+        lax.fori_loop(0, 2, step, 0)
+
+
+def final_body(groups, fars, me_ref, updated_ref, gain_ref, *refs):
+    out_ref = refs[-1]
+    me = me_ref[0]
+    width = out_ref.shape[1]
+    sums = []
+    square = 0.0
+    for g in range(len(groups)):
+        own, wide, last = refs[3 * g : 3 * g + 3]
+        total = own[0].astype(full) + wide[0].astype(full) + last[...].astype(full)
+        square = square + jnp.sum(total * total, axis=1, keepdims=True)
+        sums.append(total)
+    scale = lax.rsqrt(square / width + norm_eps)
+    for spots, total in zip(groups, sums):
+        cells = total.shape[1] // (4 * len(spots))
+        for p, (step, y) in enumerate(spots):
+            for place in range(4):
+                line = (me >> 1 & 1) ^ y
+                far = lax.rem((me >> 3) - step + fars, fars)
+                shard = far * FAR + (place >> 1) * ZL + line * Y + (place & 1)
+                columns = pl.ds(pl.multiple_of(shard * cells, cells), cells)
+                start = (p * 4 + place) * cells
+                block = total[:, start : start + cells]
+                out_ref[:, columns] = (
+                    updated_ref[:, columns].astype(full) + block * scale * gain_ref[:, columns]
+                ).astype(low)
+
+
+def flips(cells, at):
+    for axis, bit in ((0, at.core), (1, at.x), (2, at.zl)):
+        cells = jnp.where(bit == 1, jnp.flip(cells, axis), cells)
+    return cells
+
+
+def local(
+    residual_in,
+    queries,
+    keys,
+    values,
+    docs,
+    sink,
+    out_weight,
+    gate_weight,
+    up_weight,
+    down_weight,
+    conv_taps,
+    norm_gains,
+):
+    at = Place()
+    rows = queries.shape[0]
+    own, width = residual_in.shape
+    depth = gate_weight.shape[0]
+    part = gate_weight.shape[1] // 4
+    me = at.me.astype(jnp.int32).reshape(1)
+
+    def columns(base, size):
+        parts = [
+            weight[:, i * part + base : i * part + base + size]
+            for i in range(4)
+            for weight in (gate_weight, up_weight)
+        ]
+        joined = [jnp.concatenate(parts[i : i + 2], axis=1) for i in range(0, 8, 2)]
+        return jnp.stack(joined).reshape(2, 2, depth, 2 * size)
+
+    tag = jnp.broadcast_to((docs + 1).astype(low)[:, None], (rows, LANES))
+    near = jnp.concatenate([keys, values, tag], axis=1)
+    line = [(i, i + 1) for i in range(at.count - 1)]
+    before = lax.ppermute(near[rows - WINDOW :], "sp", line)
+    after = lax.ppermute(near[:WINDOW], "sp", [(j, i) for i, j in line])
+
+    split = -(-part // (2 * LANES)) * LANES
+    sizes = (split, part - split)
+    chunks = [spread(at, columns(0, sizes[0])), spread(at, columns(split, sizes[1]))]
+    down_pieces = spread(at, down_weight.reshape(2, 2, part, depth))
+
+    near = jnp.concatenate([before, near, after], axis=0)
+    half = HEAD // 2
+    freq = rope_base ** (-jnp.arange(half, dtype=full) * 2.0 / HEAD)
+    there = at.me * rows - WINDOW + jnp.arange(rows + 2 * WINDOW, dtype=jnp.int32)
+    angle = there.astype(full)[:, None] * freq[None, :]
+    cosine, sine = jnp.cos(angle), jnp.sin(angle)
+    cosine = jnp.concatenate([cosine] * 4, axis=1)
+    sine = jnp.concatenate([-sine, sine] * 2, axis=1)
+
+    def attended(index):
+        return pl.pallas_call(
+            attend_body,
+            out_shape=jax.ShapeDtypeStruct((own, width), low),
+            in_specs=[smem(), smem()] + [vmem()] * 5,
+            out_specs=vmem(),
+            scratch_shapes=[
+                pltpu.VMEM((keys.shape[1] // HEAD, own + 2 * WINDOW, LANES), low),
+                pltpu.VMEM((keys.shape[1] // HEAD, own + 2 * WINDOW, LANES), low),
+                pltpu.VMEM((own, queries.shape[1]), low),
+            ],
+            compiler_params=params,
+            cost_estimate=cost(9_000_000_000, 6_000_000),
+        )(index, sink, queries, near, cosine, sine, out_weight)
+
+    core = at.core.astype(jnp.int32).reshape(1)
+    theirs = attended(1 - core)
+    mine = attended(core)
+    given = at.other_core(theirs)
+    wide = width + LANES
+    updated, packed = pl.pallas_call(
+        normalize_body,
+        out_shape=[jax.ShapeDtypeStruct((own, width), low), jax.ShapeDtypeStruct((own, wide), low)],
+        in_specs=[smem()] + [vmem()] * 5,
+        out_specs=[vmem()] * 2,
+        compiler_params=params,
+        cost_estimate=cost(2_000_000_000, 6 * own * width * 2),
+        name="norm",
+    )(core, residual_in, mine, given, norm_gains, near)
+
+    by_z = swap(packed, ZL)
+    by_x = swap(packed, X)
+    by_xz = swap(by_z, X)
+    tokens = [packed, by_z, by_x, by_xz]
+    tokens += [at.other_core(block) for block in tokens]
+    count = len(tokens)
+
+    def spots(pieces):
+        return tuple((step, y) for step, y, _ in pieces)
+
+    taps = pick(conv_taps.reshape(3, 4, part), at.zl * 2 + at.x, 1)
+    hops = []
+    for i in range(at.count):
+        goal = i - Y + FAR if i & Y else i + Y - FAR
+        if 0 <= goal < at.count:
+            hops.append((i, goal))
+
+    sets = [[tokens[i] for i in (0, 2, 4, 6)], [tokens[i] for i in (1, 3, 5, 7)]]
+    made = {}
+    for c, (pieces, size) in enumerate(zip(chunks, sizes)):
+        for t, blocks in enumerate(sets):
+            made[c, t] = pl.pallas_call(
+                lambda *refs: product_body(spots(pieces), at.fars, 4, width, *refs),
+                out_shape=[
+                    jax.ShapeDtypeStruct((4, own, size), low),
+                    jax.ShapeDtypeStruct((4, own, size), full),
+                ],
+                grid=(2,),
+                in_specs=[smem()] + [hbm()] * (4 + len(pieces)),
+                out_specs=[pl.BlockSpec((2, own, size), lambda b: (b, 0, 0))] * 2,
+                scratch_shapes=[
+                    pltpu.VMEM((width, 2 * size), low),
+                    pltpu.VMEM((4 * own, width), low),
+                    pltpu.SemaphoreType.DMA((4 * len(pieces),)),
+                    pltpu.SemaphoreType.DMA((4,)),
+                ],
+                compiler_params=params,
+                cost_estimate=cost(16 * own * width * size, 8 * own * width),
+            )(me, *blocks, *[piece for _, _, piece in pieces])
+
+    def ends_of(t):
+        rows_ = [jnp.concatenate([made[c, t][0][:, :1], made[c, t][0][:, -1:]], axis=1) for c in (0, 1)]
+        return jnp.concatenate(rows_, axis=2).reshape(2, 2, 2, part)
+
+    edges = jnp.stack([ends_of(0), ends_of(1)], axis=2)
+    edges = flips(edges, at).transpose(2, 1, 0, 3, 4).reshape(2, 4, 2, part)
+    ends = jnp.stack([edges[:, 0, 0], edges[:, 3, 1]], axis=1)
+    side = swap(ends, Y)
+    sent = jnp.where(at.y == 1, ends[1, 1], ends[0, 0])
+    beyond = lax.ppermute(sent, "sp", hops)
+    first = jnp.where(
+        at.y == 1, jnp.stack([side[0, 1], side[1, 1]]), jnp.stack([beyond, side[0, 1]])
+    )
+    last = jnp.where(
+        at.y == 1, jnp.stack([side[1, 0], beyond]), jnp.stack([side[0, 0], side[1, 0]])
+    )
+    prev_row = jnp.concatenate([first[:, None], edges[:, :3, 1]], axis=1)
+    next_row = jnp.concatenate([edges[:, 1:, 0], last[:, None]], axis=1)
+    around = jnp.stack([prev_row, next_row], axis=2).reshape(2, 2, 2, 2, part)
+    around = flips(around.transpose(2, 1, 0, 3, 4), at)
+
+    def rows_of(*cells):
+        return pl.BlockSpec((2, 1) + cells, lambda b: (0, b, 0, 0))
+
+    kept_hidden, sent_hidden = {}, {}
+    for t in (0, 1):
+        codes = jnp.stack([block[:, width:] for block in sets[t]]).reshape(2, 2, own, LANES)
+        for c, size in enumerate(sizes):
+            columns = slice(c * split, c * split + size)
+            kept_hidden[c, t], sent_hidden[c, t] = pl.pallas_call(
+                hidden_body,
+                out_shape=[jax.ShapeDtypeStruct((2, own, size), low)] * 2,
+                grid=(2,),
+                in_specs=[
+                    rows_of(own, size),
+                    rows_of(own, size),
+                    rows_of(own, LANES),
+                    rows_of(2, size),
+                    pl.BlockSpec((3, size), lambda b: (0, 0)),
+                ],
+                out_specs=[pl.BlockSpec((1, own, size), lambda b: (b, 0, 0))] * 2,
+                compiler_params=params,
+                cost_estimate=cost(1_500_000_000, 4 * own * size * 8),
+            )(
+                made[c, t][0].reshape(2, 2, own, size),
+                made[c, t][1].reshape(2, 2, own, size),
+                codes,
+                around[:, :, t, :, columns],
+                taps[:, columns],
+            )
+
+    keys_ = [(c, t) for t in (0, 1) for c in (0, 1)]
+    inputs = [kept_hidden[key] for key in keys_]
+    inputs += [at.other_core(sent_hidden[key]) for key in keys_]
+    groups = [down_pieces[:2], down_pieces[2:]]
+    cells = 4 * depth * len(groups[0])
+    pieces = [piece for _, _, piece in down_pieces]
+    pieces += [at.other_core(piece) for piece in pieces]
+
+    def down(picked):
+        return pl.pallas_call(
+            lambda *refs: down_body(picked, *refs),
+            out_shape=[jax.ShapeDtypeStruct((2, own, cells), low)] * 2,
+            in_specs=[smem()] + [hbm()] * len(pieces) + [vmem()] * 8,
+            out_specs=[vmem()] * 2,
+            scratch_shapes=[
+                pltpu.VMEM((2, 2, part, cells), low),
+                pltpu.SemaphoreType.DMA((4 * len(pieces),)),
+            ],
+            compiler_params=params,
+            cost_estimate=cost(count * own * part * width, 6 * own * width),
+        )(me, *pieces, *inputs)
+
+    sent_x, sent_z = down(((2, 3), (1, 3), (), ()))
+    kept_x, kept_z = down(((0, 1), (0, 2), (), ()))
+    wide_x = swap(sent_x, X)
+    wide_z = swap(sent_z, ZL)
+    finals = []
+    for kept, wide_sum, bit in ((kept_x, wide_x, ZL), (kept_z, wide_z, X)):
+        sent = (kept[1].astype(full) + wide_sum[1].astype(full)).astype(low)
+        finals += [kept, wide_sum, swap(sent, bit)]
+
+    def blocks(i):
+        cells = finals[i].shape[-1]
+        if i % 3 == 2:
+            return pl.BlockSpec((own // 4, cells), lambda s: (s, 0))
+        return pl.BlockSpec((1, own // 4, cells), lambda s: (0, s, 0))
+
+    whole = pl.BlockSpec((own // 4, width), lambda s: (s, 0))
+    return pl.pallas_call(
+        lambda *refs: final_body([spots(pieces) for pieces in groups], at.fars, *refs),
+        out_shape=jax.ShapeDtypeStruct((own, width), low),
+        grid=(4,),
+        in_specs=[smem(), whole, pl.BlockSpec((1, width), lambda s: (0, 0))]
+        + [blocks(i) for i in range(len(finals))],
+        out_specs=whole,
+        compiler_params=params,
+        cost_estimate=cost(own * width * 10, own * width * 14),
+        name="final",
+    )(me, updated, norm_gains[2:3], *finals)
+
+
+def grouped(mesh, shapes):
+    sp, tp = mesh.shape["sp"], mesh.shape["tp"]
+    width, hidden = shapes[7].shape
+    fits = tp == 2 and sp == 2 * FAR
+    return fits and width // sp % LANES == 0 and hidden // tp // 4 % 16 == 0
+
+
+def staged(*arrays):
+    return local(*arrays)
+
+
 def solution(mesh):
     in_specs = (
         P(("sp", "tp"), None),
@@ -160,4 +726,16 @@
         P(),
     )
     out_specs = P(("sp", "tp"), None)
-    return jax.shard_map(local, mesh=mesh, in_specs=in_specs, out_specs=out_specs, check_vma=False)
+
+    def run(*arrays):
+        fits = grouped(mesh, arrays)
+        step = jax.shard_map(
+            staged if fits else plain,
+            mesh=mesh,
+            in_specs=in_specs,
+            out_specs=out_specs,
+            check_vma=False,
+        )
+        return step(*arrays)
+
+    return run

time: 612 us -> 285 us (0.47)
  waiting for transfers between devices: 487 us -> 111 us
  Pallas kernels: 0 us -> 91.6 us
  matrix products: 56.8 us -> 0 us
  local copies, waits for them, and re-layouts: 8.33 us -> 26.3 us
  starting transfers between devices: 23 us -> 40 us
  between operations: 13.9 us -> 0.74 us
  other arithmetic: 22.6 us -> 11.4 us
    all_gather x4 -> x0, waiting for transfers between devices: 457 us -> none  [the longest x1 160 us: local(): lax.all_gather(down_weight, 'sp', axis=1, tiled=True)]
    ppermute x8 -> x39, waiting for transfers between devices: 4.55 us -> 111 us  [the longest x20 82 us: swap(): lax.ppermute(cells, 'sp', [(i, i ^ bit) for i in range(lax.axis_size('sp'...]
    pallas_call x0 -> x14, Pallas kernels: none -> 91.6 us  [the longest x4 30.8 us: local(): pl.pallas_call(lambda *refs: product_body(spots(pieces), at.fars, 4, widt...]
    dot_general x5 -> x0, matrix products: 56.8 us -> none  [the longest x1 25 us: local(): jnp.dot(hidden, lax.all_gather(down_weight, 'sp', axis=1, tiled=True), pr...]
    reduce_scatter x2 -> x0, waiting for transfers between devices: 23.4 us -> none  [the longest x1 15.3 us: local(): lax.psum_scatter(jnp.dot(attended, out_weight, preferred_element_type=jnp...]
    ppermute x8 -> x39, starting transfers between devices: 22.7 us -> 40 us  [the longest x20 28.5 us: swap(): lax.ppermute(cells, 'sp', [(i, i ^ bit) for i in range(lax.axis_size('sp'...]
    reduce_sum x4 -> x0, other arithmetic: 10.2 us -> none  [the longest x1 5.29 us: attend(): total = jnp.sum(weights, axis=-1) + jnp.exp(sink_group - top)]
  transfers between devices with their start and end apart: 14 -> 39, of which waited for: 8 -> 15; matrix products, arithmetic and copies ran while one was open for 6% -> 11% of each run, Pallas kernels for 0% -> 28%
where the time goes in v1:
time: 285 us; the launch traced here: 281 us
  waiting for transfers between devices  111 us (39%)
  Pallas kernels  91.6 us (32%)
  starting transfers between devices  40 us (14%)
  local copies, waits for them, and re-layouts  26.3 us (9%)
  other arithmetic  11.4 us (4%)
    ppermute x20, waiting for transfers between devices, swap(): lax.ppermute(cells, 'sp', [(i, i ^ bit) for i in range(lax.axis_size('sp'...  82 us
    pallas_call x4, Pallas kernels, local(): pl.pallas_call(lambda *refs: product_body(spots(pieces), at.fars, 4, widt...  30.8 us
    ppermute x20, starting transfers between devices, swap(): lax.ppermute(cells, 'sp', [(i, i ^ bit) for i in range(lax.axis_size('sp'...  28.5 us
    ppermute x3, waiting for transfers between devices, far_shift(): return lax.ppermute(cells, 'sp', hops)  25 us
    pallas_call x2, Pallas kernels, attended(): pl.pallas_call(attend_body, out_shape=jax.ShapeDtypeStruct((own, width),...  21.6 us
    pallas_call x2, Pallas kernels, down(): pl.pallas_call(lambda *refs: down_body(picked, *refs), out_shape=[jax.Sha...  17.8 us
    pallas_call x4, Pallas kernels, local(): pl.pallas_call(hidden_body, out_shape=[jax.ShapeDtypeStruct((2, own, size...  12.7 us
    another operation x8, local copies, waits for them, and re-layouts, local(): jnp.stack([block[:, width:] for block in sets[t]]).reshape(2, 2, own, LANES)  5.92 us
  transfers between devices with their start and end apart: 39, of which 15 were waited for; matrix products, arithmetic and copies ran while one was open for 11% of the time, Pallas kernels for 28%

profile of v1, /device:TPU:0, one launch (start us, length us, event | category | flops | bytes accessed | tf_op | source)
XLA Modules:
  0.0 281.0 jit_solution(18283988738795452545)
XLA Ops:
  3.6 3.0 %collective-permute-start.20 = (bf16[2,128,640]{2,1,0:T(8,128)(2,1)}, bf16[2,128,640]{2,1,0:T(8,128)(2,1)}, u32[]{:S(2)}, u32[]{:S(2)}) collective-permute-start(bf16[2,128,640]{2,1,0:T(8,128)(2,1)} %dynamic-slice_bitcast_fusion.2), channel_id=1, source_target_pairs={{0,2},{2,0},{4,6},{6,4},{8,10},{10,8},{12,14},{14,12},{16,18},{18,... | collective-permute-start | bytes 983048 | tf_op jit(solution)/shard_map/ppermute | solution.py:174
  24.5 10.9 %shard_map.119 = bf16[256,2048]{1,0:T(8,128)(2,1)} custom-call(s32[1]{0:T(128)S(6)} %sub.9.half_ref, f32[16]{0:T(128)} %sink_ref.3, bf16[512,1024]{1,0:T(8,128)(2,1)} %q_ref.3, bf16[768,640]{1,0:T(8,128)(2,1)} %pad_maximum_fusion.near_ref, f32[768,128]{1,0:T(8,128)} %get-tuple-element.102.cos_ref, f32[768,128]{1,0:T(8,128)} %get-tuple-element.103.sin_ref, ...), custom_call_target="tpu_custom_call" | custom-call | flops 8999999488 | bytes 6000000 | tf_op jit(solution)/shard_map/pallas_call | solution.py:531
  35.4 10.7 %shard_map.118.own_ref = bf16[256,2048]{1,0:T(8,128)(2,1)} custom-call(s32[1]{0:T(128)} %bitcast.1.half_ref.core_ref, f32[16]{0:T(128)} %sink_ref.3, bf16[512,1024]{1,0:T(8,128)(2,1)} %q_ref.3, bf16[768,640]{1,0:T(8,128)(2,1)} %pad_maximum_fusion.near_ref, f32[768,128]{1,0:T(8,128)} %get-tuple-element.102.cos_ref, f32[768,128]{1,0:T(8,128)} %get-tuple-element.103.sin_ref, ...), custom_call_target="tpu_custom_call" | custom-call | flops 8999999488 | bytes 6000000 | tf_op jit(solution)/shard_map/pallas_call | solution.py:531
  51.7 4.3 %norm.1 = (bf16[256,2048]{1,0:T(8,128)(2,1)}, bf16[256,2176]{1,0:T(8,128)(2,1)}) custom-call(s32[1]{0:T(128)} %bitcast.1.half_ref.core_ref, bf16[256,2048]{1,0:T(8,128)(2,1)} %residual_ref.1, bf16[256,2048]{1,0:T(8,128)(2,1)} %shard_map.118.own_ref, bf16[256,2048]{1,0:T(8,128)(2,1)} %collective-permute-done.2.given_ref, f32[3,2048]{1,0:T(4,128)} %gains_ref.1, ...), custom_call_target="tpu_custom_call" | custom-call | flops 2000000000 | bytes 6291456 | tf_op jit(solution)/shard_map/norm/pallas_call | solution.py:550
  63.6 14.9 %collective-permute-done.4 = bf16[2,704,128]{2,1,0:T(8,128)(2,1)} collective-permute-done((bf16[2,704,128]{2,1,0:T(8,128)(2,1)S(1)}, bf16[2,704,128]{2,1,0:T(8,128)(2,1)}, u32[]{:S(2)}, u32[]{:S(2)}) %collective-permute-start.4) | collective-permute-done | bytes 360480 | tf_op jit(solution)/shard_map/ppermute | solution.py:174
  81.3 5.6 %collective-permute-done.16 = bf16[2,128,768]{2,1,0:T(8,128)(2,1)S(1)} collective-permute-done((bf16[2,128,768]{2,1,0:T(8,128)(2,1)S(1)}, bf16[2,128,768]{2,1,0:T(8,128)(2,1)S(1)}, u32[]{:S(2)}, u32[]{:S(2)}) %collective-permute-start.16) | collective-permute-done | bytes 393248 | tf_op jit(solution)/shard_map/ppermute | solution.py:174
  87.0 5.1 %collective-permute-done.23.refs_7_ = bf16[4,128,640]{2,1,0:T(8,128)(2,1)} collective-permute-done((bf16[4,128,640]{2,1,0:T(8,128)(2,1)S(1)}, bf16[4,128,640]{2,1,0:T(8,128)(2,1)}, u32[]{:S(2)}, u32[]{:S(2)}) %collective-permute-start.23) | collective-permute-done | bytes 655392 | tf_op jit(solution)/shard_map/ppermute | solution.py:197
  92.1 3.9 %collective-permute-done.22.refs_6_ = bf16[4,128,640]{2,1,0:T(8,128)(2,1)S(1)} collective-permute-done((bf16[4,128,640]{2,1,0:T(8,128)(2,1)S(1)}, bf16[4,128,640]{2,1,0:T(8,128)(2,1)S(1)}, u32[]{:S(2)}, u32[]{:S(2)}) %collective-permute-start.22) | collective-permute-done | bytes 655392 | tf_op jit(solution)/shard_map/ppermute | solution.py:174
  101.1 27.8 %collective-permute-done.25.refs_1_ = bf16[256,2176]{1,0:T(8,128)(2,1)} collective-permute-done((bf16[256,2176]{1,0:T(8,128)(2,1)}, bf16[256,2176]{1,0:T(8,128)(2,1)}, u32[]{:S(2)}, u32[]{:S(2)}) %collective-permute-start.25) | collective-permute-done | bytes 1114144 | tf_op jit(solution)/shard_map/ppermute | solution.py:174
  138.6 7.7 %shard_map.121 = (bf16[4,256,320]{2,1,0:T(8,128)(2,1)}, f32[4,256,320]{2,1,0:T(8,128)}) custom-call(s32[1]{0:T(128)} %bitcast.refs_0_, bf16[256,2176]{1,0:T(8,128)(2,1)} %get-tuple-element.28.refs_1_, bf16[256,2176]{1,0:T(8,128)(2,1)} %collective-permute-done.12.refs_2_, bf16[256,2176]{1,0:T(8,128)(2,1)} %collective-permute-done.13.refs_3_, ...), custom_call_target="tpu_custom_call" | custom-call | flops 2684354560 | bytes 4194304 | tf_op jit(solution)/shard_map/pallas_call | solution.py:581
  146.3 19.8 %collective-permute-done.6.refs_3_ = bf16[4,704,128]{2,1,0:T(8,128)(2,1)} collective-permute-done((bf16[4,704,128]{2,1,0:T(8,128)(2,1)S(1)}, bf16[4,704,128]{2,1,0:T(8,128)(2,1)}, u32[]{:S(2)}, u32[]{:S(2)}) %collective-permute-start.6) | collective-permute-done | bytes 720928 | tf_op jit(solution)/shard_map/ppermute | solution.py:197
  166.2 5.1 %collective-permute-done.19.refs_8_ = bf16[4,128,768]{2,1,0:T(8,128)(2,1)} collective-permute-done((bf16[4,128,768]{2,1,0:T(8,128)(2,1)}, bf16[4,128,768]{2,1,0:T(8,128)(2,1)}, u32[]{:S(2)}, u32[]{:S(2)}) %collective-permute-start.19) | collective-permute-done | bytes 786464 | tf_op jit(solution)/shard_map/ppermute | solution.py:174
  171.8 7.7 %shard_map.120 = (bf16[4,256,384]{2,1,0:T(8,128)(2,1)}, f32[4,256,384]{2,1,0:T(8,128)}) custom-call(s32[1]{0:T(128)} %bitcast.refs_0_, bf16[256,2176]{1,0:T(8,128)(2,1)} %get-tuple-element.28.refs_1_, bf16[256,2176]{1,0:T(8,128)(2,1)} %collective-permute-done.12.refs_2_, bf16[256,2176]{1,0:T(8,128)(2,1)} %collective-permute-done.13.refs_3_, ...), custom_call_target="tpu_custom_call" | custom-call | flops 3221225472 | bytes 4194304 | tf_op jit(solution)/shard_map/pallas_call | solution.py:581
  184.6 7.7 %shard_map.122 = (bf16[4,256,384]{2,1,0:T(8,128)(2,1)}, f32[4,256,384]{2,1,0:T(8,128)}) custom-call(s32[1]{0:T(128)} %bitcast.refs_0_, bf16[256,2176]{1,0:T(8,128)(2,1)} %collective-permute-done.25.refs_1_, bf16[256,2176]{1,0:T(8,128)(2,1)} %copy-done.15, bf16[256,2176]{1,0:T(8,128)(2,1)} %collective-permute-done.27.refs_3_, bf16[256,2176]{1,0:T(8,128)(2,1)} %copy-done.16, ...), custom_call_target="tpu_custom_call" | custom-call | flops 3221225472 | bytes 4194304 | tf_op jit(solution)/shard_map/pallas_call | solution.py:581
  193.1 7.8 %shard_map.123 = (bf16[4,256,320]{2,1,0:T(8,128)(2,1)}, f32[4,256,320]{2,1,0:T(8,128)}) custom-call(s32[1]{0:T(128)} %bitcast.refs_0_, bf16[256,2176]{1,0:T(8,128)(2,1)} %collective-permute-done.25.refs_1_, bf16[256,2176]{1,0:T(8,128)(2,1)} %copy-done.15, bf16[256,2176]{1,0:T(8,128)(2,1)} %collective-permute-done.27.refs_3_, bf16[256,2176]{1,0:T(8,128)(2,1)} %copy-done.16, ...), custom_call_target="tpu_custom_call" | custom-call | flops 2684354560 | bytes 4194304 | tf_op jit(solution)/shard_map/pallas_call | solution.py:581
  206.5 3.2 %shard_map.126 = (bf16[2,256,384]{2,1,0:T(8,128)(2,1)}, bf16[2,256,384]{2,1,0:T(8,128)(2,1)}) custom-call(bf16[2,2,256,384]{3,2,1,0:T(8,128)(2,1)} %bitcast.133, f32[2,2,256,384]{3,2,1,0:T(8,128)} %bitcast.137, bf16[2,2,256,128]{3,2,1,0:T(8,128)(2,1)} %bitcast.115, bf16[2,2,2,384]{3,2,1,0:T(2,128)(2,1)} %get-tuple-element.89.around_ref, ...), custom_call_target="tpu_custom_call" | custom-call | flops 1500000000 | bytes 3145728 | tf_op jit(solution)/shard_map/pallas_call | solution.py:629
  210.3 3.2 %shard_map.127 = (bf16[2,256,320]{2,1,0:T(8,128)(2,1)}, bf16[2,256,320]{2,1,0:T(8,128)(2,1)}) custom-call(bf16[2,2,256,320]{3,2,1,0:T(8,128)(2,1)} %bitcast.132, f32[2,2,256,320]{3,2,1,0:T(8,128)} %bitcast.136, bf16[2,2,256,128]{3,2,1,0:T(8,128)(2,1)} %bitcast.116, bf16[2,2,2,320]{3,2,1,0:T(2,128)(2,1)} %get-tuple-element.87.around_ref, ...), custom_call_target="tpu_custom_call" | custom-call | flops 1500000000 | bytes 2621440 | tf_op jit(solution)/shard_map/pallas_call | solution.py:629
  213.4 3.2 %shard_map.124 = (bf16[2,256,384]{2,1,0:T(8,128)(2,1)}, bf16[2,256,384]{2,1,0:T(8,128)(2,1)}) custom-call(bf16[2,2,256,384]{3,2,1,0:T(8,128)(2,1)} %bitcast.131, f32[2,2,256,384]{3,2,1,0:T(8,128)} %bitcast.135, bf16[2,2,256,128]{3,2,1,0:T(8,128)(2,1)} %bitcast.113, bf16[2,2,2,384]{3,2,1,0:T(2,128)(2,1)} %get-tuple-element.90.around_ref, ...), custom_call_target="tpu_custom_call" | custom-call | flops 1500000000 | bytes 3145728 | tf_op jit(solution)/shard_map/pallas_call | solution.py:629
  217.2 3.2 %shard_map.125 = (bf16[2,256,320]{2,1,0:T(8,128)(2,1)}, bf16[2,256,320]{2,1,0:T(8,128)(2,1)}) custom-call(bf16[2,2,256,320]{3,2,1,0:T(8,128)(2,1)} %bitcast.130, f32[2,2,256,320]{3,2,1,0:T(8,128)} %bitcast.134, bf16[2,2,256,128]{3,2,1,0:T(8,128)(2,1)} %bitcast.114, bf16[2,2,2,320]{3,2,1,0:T(2,128)(2,1)} %get-tuple-element.88.around_ref, ...), custom_call_target="tpu_custom_call" | custom-call | flops 1500000000 | bytes 2621440 | tf_op jit(solution)/shard_map/pallas_call | solution.py:629
  224.5 8.9 %shard_map.129 = (bf16[2,256,1024]{2,1,0:T(8,128)(2,1)}, bf16[2,256,1024]{2,1,0:T(8,128)(2,1)}) custom-call(s32[1]{0:T(128)} %bitcast.refs_0_, bf16[4,704,128]{2,1,0:T(8,128)(2,1)} %copy-done.9, bf16[4,704,128]{2,1,0:T(8,128)(2,1)} %collective-permute-done.5.refs_2_, bf16[4,704,128]{2,1,0:T(8,128)(2,1)} %collective-permute-done.6.refs_3_, ...), custom_call_target="tpu_custom_call" | custom-call | flops 2952790016 | bytes 3145728 | tf_op jit(solution)/shard_map/pallas_call | solution.py:660
  236.5 8.9 %shard_map.128 = (bf16[2,256,1024]{2,1,0:T(8,128)(2,1)}, bf16[2,256,1024]{2,1,0:T(8,128)(2,1)}) custom-call(s32[1]{0:T(128)} %bitcast.refs_0_, bf16[4,704,128]{2,1,0:T(8,128)(2,1)} %copy-done.9, bf16[4,704,128]{2,1,0:T(8,128)(2,1)} %collective-permute-done.5.refs_2_, bf16[4,704,128]{2,1,0:T(8,128)(2,1)} %collective-permute-done.6.refs_3_, ...), custom_call_target="tpu_custom_call" | custom-call | flops 2952790016 | bytes 3145728 | tf_op jit(solution)/shard_map/pallas_call | solution.py:660
  245.4 14.2 %collective-permute-done.37.refs_7_ = bf16[2,256,1024]{2,1,0:T(8,128)(2,1)S(1)} collective-permute-done((bf16[2,256,1024]{2,1,0:T(8,128)(2,1)}, bf16[2,256,1024]{2,1,0:T(8,128)(2,1)S(1)}, u32[]{:S(2)}, u32[]{:S(2)}) %collective-permute-start.37) | collective-permute-done | bytes 1048608 | tf_op jit(solution)/shard_map/ppermute | solution.py:174
  265.4 9.2 %collective-permute-done.38.refs_8_ = bf16[256,1024]{1,0:T(8,128)(2,1)S(1)} collective-permute-done((bf16[256,1024]{1,0:T(8,128)(2,1)S(1)}, bf16[256,1024]{1,0:T(8,128)(2,1)S(1)}, u32[]{:S(2)}, u32[]{:S(2)}) %collective-permute-start.38) | collective-permute-done | bytes 524320 | tf_op jit(solution)/shard_map/ppermute | solution.py:174
  276.5 4.5 %final.1 = bf16[256,2048]{1,0:T(8,128)(2,1)} custom-call(s32[1]{0:T(128)} %bitcast.refs_0_, bf16[256,2048]{1,0:T(8,128)(2,1)} %get-tuple-element.27.refs_1_, f32[1,2048]{1,0:T(1,128)} %slice.173.refs_2_, bf16[2,256,1024]{2,1,0:T(8,128)(2,1)} %get-tuple-element.45.refs_3_, bf16[2,256,1024]{2,1,0:T(8,128)(2,1)} %copy-done.1, bf16[256,1024]{1,0:T(8,128)(2,1)} %copy-done.13, ...), custom_call_target="tpu_custom_call" | custom-call | flops 5242880 | bytes 7340032 | tf_op jit(solution)/shard_map/final/pallas_call | solution.py:689
  (203 shorter events, 80.0 us)
Async XLA Ops:
  3.6 42.5 %collective-permute-start.20 = (bf16[2,128,640]{2,1,0:T(8,128)(2,1)}, bf16[2,128,640]{2,1,0:T(8,128)(2,1)}, u32[]{:S(2)}, u32[]{:S(2)}) collective-permute-start(bf16[2,128,640]{2,1,0:T(8,128)(2,1)} %dynamic-slice_bitcast_fusion.2), channel_id=1, source_target_pairs={{0,2},{2,0},{4,6},{6,4},{8,10},{10,8},{12,14},{14,12},{16,18},{18,... | collective-permute-start | bytes 983048 | tf_op jit(solution)/shard_map/ppermute | solution.py:174
  12.6 38.1 %collective-permute-start.15 = (bf16[2,128,768]{2,1,0:T(8,128)(2,1)}, bf16[2,128,768]{2,1,0:T(8,128)(2,1)}, u32[]{:S(2)}, u32[]{:S(2)}) collective-permute-start(bf16[2,128,768]{2,1,0:T(8,128)(2,1)} %dynamic-slice_bitcast_fusion), channel_id=1, source_target_pairs={{0,2},{2,0},{4,6},{6,4},{8,10},{10,8},{12,14},{14,12},{16,18},{18,... | collective-permute-start | bytes 1179656 | tf_op jit(solution)/shard_map/ppermute | solution.py:174
  16.3 33.1 %collective-permute-start.3 = (bf16[2,704,128]{2,1,0:T(8,128)(2,1)}, bf16[2,704,128]{2,1,0:T(8,128)(2,1)}, u32[]{:S(2)}, u32[]{:S(2)}) collective-permute-start(bf16[2,704,128]{2,1,0:T(8,128)(2,1)} %dynamic-slice_bitcast_fusion.1), channel_id=1, source_target_pairs={{0,2},{2,0},{4,6},{6,4},{8,10},{10,8},{12,14},{14,12},{16,18},{18,... | collective-permute-start | bytes 1081352 | tf_op jit(solution)/shard_map/ppermute | solution.py:174
  35.4 16.3 %collective-permute-start.2 = (bf16[256,2048]{1,0:T(8,128)(2,1)}, bf16[256,2048]{1,0:T(8,128)(2,1)}, u32[]{:S(2)}, u32[]{:S(2)}) collective-permute-start(bf16[256,2048]{1,0:T(8,128)(2,1)} %shard_map.119), channel_id=1, source_target_pairs={{0,1},{1,0},{2,3},{3,2},{4,5},{5,4},{6,7},{7,6},{8,9},{9,8},{10,11... | collective-permute-start | bytes 3145736 | tf_op jit(solution)/shard_map/ppermute | solution.py:193
  50.5 28.0 %collective-permute-start.4 = (bf16[2,704,128]{2,1,0:T(8,128)(2,1)S(1)}, bf16[2,704,128]{2,1,0:T(8,128)(2,1)}, u32[]{:S(2)}, u32[]{:S(2)}) collective-permute-start(bf16[2,704,128]{2,1,0:T(8,128)(2,1)S(1)} %pad_maximum_fusion.9), channel_id=1, source_target_pairs={{0,8},{2,10},{4,12},{6,14},{8,0},{10,2},{12,4},{14,6},{16,24},{18,... | collective-permute-start | bytes 1081352 | tf_op jit(solution)/shard_map/ppermute | solution.py:174
  55.9 42.7 %collective-permute-start.12 = (bf16[256,2176]{1,0:T(8,128)(2,1)}, bf16[256,2176]{1,0:T(8,128)(2,1)}, u32[]{:S(2)}, u32[]{:S(2)}) collective-permute-start(bf16[256,2176]{1,0:T(8,128)(2,1)} %get-tuple-element.28.refs_1_), channel_id=1, source_target_pairs={{0,2},{2,0},{4,6},{6,4},{8,10},{10,8},{12,14},{14,12},{16,18},{18,... | collective-permute-start | bytes 3342344 | tf_op jit(solution)/shard_map/ppermute | solution.py:174
  58.8 28.1 %collective-permute-start.16 = (bf16[2,128,768]{2,1,0:T(8,128)(2,1)S(1)}, bf16[2,128,768]{2,1,0:T(8,128)(2,1)S(1)}, u32[]{:S(2)}, u32[]{:S(2)}) collective-permute-start(bf16[2,128,768]{2,1,0:T(8,128)(2,1)S(1)} %pad_maximum_fusion.8), channel_id=1, source_target_pairs={{0,8},{2,10},{4,12},{6,14},{8,0},{10,2},{12,4},{14,6},{16,24},{18,... | collective-permute-start | bytes 1179656 | tf_op jit(solution)/shard_map/ppermute | solution.py:174
  60.5 31.6 %collective-permute-start.23 = (bf16[4,128,640]{2,1,0:T(8,128)(2,1)S(1)}, bf16[4,128,640]{2,1,0:T(8,128)(2,1)}, u32[]{:S(2)}, u32[]{:S(2)}) collective-permute-start(bf16[4,128,640]{2,1,0:T(8,128)(2,1)S(1)} %pad_maximum_fusion.5.refs_5_), channel_id=1, source_target_pairs={{0,16},{2,18},{4,20},{6,22},{8,24},{10,26},{12,28},{14,30},{16,0},... | collective-permute-start | bytes 1966088 | tf_op jit(solution)/shard_map/ppermute | solution.py:197
  63.2 65.7 %collective-permute-start.25 = (bf16[256,2176]{1,0:T(8,128)(2,1)}, bf16[256,2176]{1,0:T(8,128)(2,1)}, u32[]{:S(2)}, u32[]{:S(2)}) collective-permute-start(bf16[256,2176]{1,0:T(8,128)(2,1)} %get-tuple-element.28.refs_1_), channel_id=1, source_target_pairs={{0,8},{2,10},{4,12},{6,14},{8,0},{10,2},{12,4},{14,6},{16,24},{18,... | collective-permute-start | bytes 3342344 | tf_op jit(solution)/shard_map/ppermute | solution.py:174
  78.6 17.4 %collective-permute-start.22 = (bf16[4,128,640]{2,1,0:T(8,128)(2,1)S(1)}, bf16[4,128,640]{2,1,0:T(8,128)(2,1)S(1)}, u32[]{:S(2)}, u32[]{:S(2)}) collective-permute-start(bf16[4,128,640]{2,1,0:T(8,128)(2,1)S(1)} %pad_maximum_fusion.5.refs_5_), channel_id=1, source_target_pairs={{0,4},{2,6},{4,0},{6,2},{8,12},{10,14},{12,8},{14,10},{16,20},{18,... | collective-permute-start | bytes 1966088 | tf_op jit(solution)/shard_map/ppermute | solution.py:174
  86.9 47.0 %collective-permute-start.13 = (bf16[256,2176]{1,0:T(8,128)(2,1)}, bf16[256,2176]{1,0:T(8,128)(2,1)}, u32[]{:S(2)}, u32[]{:S(2)}) collective-permute-start(bf16[256,2176]{1,0:T(8,128)(2,1)} %get-tuple-element.28.refs_1_), channel_id=1, source_target_pairs={{0,1},{1,0},{2,3},{3,2},{4,5},{5,4},{6,7},{7,6},{8,9},{9,8},{10,11... | collective-permute-start | bytes 3342344 | tf_op jit(solution)/shard_map/ppermute | solution.py:193
  92.1 40.1 %collective-permute-start.18 = (bf16[4,128,768]{2,1,0:T(8,128)(2,1)S(1)}, bf16[4,128,768]{2,1,0:T(8,128)(2,1)}, u32[]{:S(2)}, u32[]{:S(2)}) collective-permute-start(bf16[4,128,768]{2,1,0:T(8,128)(2,1)S(1)} %pad_maximum_fusion.2.refs_5_), channel_id=1, source_target_pairs={{0,16},{2,18},{4,20},{6,22},{8,24},{10,26},{12,28},{14,30},{16,0},... | collective-permute-start | bytes 2359304 | tf_op jit(solution)/shard_map/ppermute | solution.py:197
  96.8 37.1 %collective-permute-start.24 = (bf16[4,128,640]{2,1,0:T(8,128)(2,1)}, bf16[4,128,640]{2,1,0:T(8,128)(2,1)}, u32[]{:S(2)}, u32[]{:S(2)}) collective-permute-start(bf16[4,128,640]{2,1,0:T(8,128)(2,1)} %collective-permute-done.23.refs_7_), channel_id=1, source_target_pairs={{0,4},{2,6},{4,0},{6,2},{8,12},{10,14},{12,8},{14,10},{16,20},{18,... | collective-permute-start | bytes 1966088 | tf_op jit(solution)/shard_map/ppermute | solution.py:174
  98.7 39.8 %collective-permute-start.14 = (bf16[256,2176]{1,0:T(8,128)(2,1)}, bf16[256,2176]{1,0:T(8,128)(2,1)}, u32[]{:S(2)}, u32[]{:S(2)}) collective-permute-start(bf16[256,2176]{1,0:T(8,128)(2,1)} %collective-permute-done.12.refs_2_), channel_id=1, source_target_pairs={{0,1},{1,0},{2,3},{3,2},{4,5},{5,4},{6,7},{7,6},{8,9},{9,8},{10,11... | collective-permute-start | bytes 3342344 | tf_op jit(solution)/shard_map/ppermute | solution.py:193
  128.9 42.5 %collective-permute-start.26 = (bf16[256,2176]{1,0:T(8,128)(2,1)}, bf16[256,2176]{1,0:T(8,128)(2,1)S(1)}, u32[]{:S(2)}, u32[]{:S(2)}) collective-permute-start(bf16[256,2176]{1,0:T(8,128)(2,1)} %collective-permute-done.25.refs_1_), channel_id=1, source_target_pairs={{0,2},{2,0},{4,6},{6,4},{8,10},{10,8},{12,14},{14,12},{16,18},{18,... | collective-permute-start | bytes 3342344 | tf_op jit(solution)/shard_map/ppermute | solution.py:174
  132.2 33.9 %collective-permute-start.6 = (bf16[4,704,128]{2,1,0:T(8,128)(2,1)S(1)}, bf16[4,704,128]{2,1,0:T(8,128)(2,1)}, u32[]{:S(2)}, u32[]{:S(2)}) collective-permute-start(bf16[4,704,128]{2,1,0:T(8,128)(2,1)S(1)} %pad_maximum_fusion.3.refs_1_), channel_id=1, source_target_pairs={{0,16},{2,18},{4,20},{6,22},{8,24},{10,26},{12,28},{14,30},{16,0},... | collective-permute-start | bytes 2162696 | tf_op jit(solution)/shard_map/ppermute | solution.py:197
  133.9 32.2 %collective-permute-start.17 = (bf16[4,128,768]{2,1,0:T(8,128)(2,1)S(1)}, bf16[4,128,768]{2,1,0:T(8,128)(2,1)}, u32[]{:S(2)}, u32[]{:S(2)}) collective-permute-start(bf16[4,128,768]{2,1,0:T(8,128)(2,1)S(1)} %pad_maximum_fusion.2.refs_5_), channel_id=1, source_target_pairs={{0,4},{2,6},{4,0},{6,2},{8,12},{10,14},{12,8},{14,10},{16,20},{18,... | collective-permute-start | bytes 2359304 | tf_op jit(solution)/shard_map/ppermute | solution.py:174
  133.9 37.4 %collective-permute-start.19 = (bf16[4,128,768]{2,1,0:T(8,128)(2,1)}, bf16[4,128,768]{2,1,0:T(8,128)(2,1)}, u32[]{:S(2)}, u32[]{:S(2)}) collective-permute-start(bf16[4,128,768]{2,1,0:T(8,128)(2,1)} %collective-permute-done.18.refs_7_), channel_id=1, source_target_pairs={{0,4},{2,6},{4,0},{6,2},{8,12},{10,14},{12,8},{14,10},{16,20},{18,... | collective-permute-start | bytes 2359304 | tf_op jit(solution)/shard_map/ppermute | solution.py:174
  138.5 65.8 %collective-permute-start.5 = (bf16[4,704,128]{2,1,0:T(8,128)(2,1)S(1)}, bf16[4,704,128]{2,1,0:T(8,128)(2,1)}, u32[]{:S(2)}, u32[]{:S(2)}) collective-permute-start(bf16[4,704,128]{2,1,0:T(8,128)(2,1)S(1)} %pad_maximum_fusion.3.refs_1_), channel_id=1, source_target_pairs={{0,4},{2,6},{4,0},{6,2},{8,12},{10,14},{12,8},{14,10},{16,20},{18,... | collective-permute-start | bytes 2162696 | tf_op jit(solution)/shard_map/ppermute | solution.py:174
  166.1 50.5 %collective-permute-start.8 = (bf16[4,704,128]{2,1,0:T(8,128)(2,1)S(1)}, bf16[4,704,128]{2,1,0:T(8,128)(2,1)}, u32[]{:S(2)}, u32[]{:S(2)}) collective-permute-start(bf16[4,704,128]{2,1,0:T(8,128)(2,1)S(1)} %pad_maximum_fusion.3.refs_1_), channel_id=1, source_target_pairs={{0,1},{1,0},{2,3},{3,2},{4,5},{5,4},{6,7},{7,6},{8,9},{9,8},{10,11... | collective-permute-start | bytes 2162696 | tf_op jit(solution)/shard_map/ppermute | solution.py:193
  166.1 38.6 %collective-permute-start.7 = (bf16[4,704,128]{2,1,0:T(8,128)(2,1)}, bf16[4,704,128]{2,1,0:T(8,128)(2,1)}, u32[]{:S(2)}, u32[]{:S(2)}) collective-permute-start(bf16[4,704,128]{2,1,0:T(8,128)(2,1)} %collective-permute-done.6.refs_3_), channel_id=1, source_target_pairs={{0,4},{2,6},{4,0},{6,2},{8,12},{10,14},{12,8},{14,10},{16,20},{18,... | collective-permute-start | bytes 2162696 | tf_op jit(solution)/shard_map/ppermute | solution.py:174
  204.9 16.1 %collective-permute-start.11 = (bf16[4,704,128]{2,1,0:T(8,128)(2,1)}, bf16[4,704,128]{2,1,0:T(8,128)(2,1)S(1)}, u32[]{:S(2)}, u32[]{:S(2)}) collective-permute-start(bf16[4,704,128]{2,1,0:T(8,128)(2,1)} %collective-permute-done.7.refs_4_), channel_id=1, source_target_pairs={{0,1},{1,0},{2,3},{3,2},{4,5},{5,4},{6,7},{7,6},{8,9},{9,8},{10,11... | collective-permute-start | bytes 2162696 | tf_op jit(solution)/shard_map/ppermute | solution.py:193
  233.4 26.2 %collective-permute-start.37 = (bf16[2,256,1024]{2,1,0:T(8,128)(2,1)}, bf16[2,256,1024]{2,1,0:T(8,128)(2,1)S(1)}, u32[]{:S(2)}, u32[]{:S(2)}) collective-permute-start(bf16[2,256,1024]{2,1,0:T(8,128)(2,1)} %get-tuple-element.48), channel_id=1, source_target_pairs={{0,8},{2,10},{4,12},{6,14},{8,0},{10,2},{12,4},{14,6},{16,24},{18,... | collective-permute-start | bytes 3145736 | tf_op jit(solution)/shard_map/ppermute | solution.py:174
  235.9 26.1 %collective-permute-start.35 = (bf16[2,256,1024]{2,1,0:T(8,128)(2,1)}, bf16[2,256,1024]{2,1,0:T(8,128)(2,1)S(1)}, u32[]{:S(2)}, u32[]{:S(2)}) collective-permute-start(bf16[2,256,1024]{2,1,0:T(8,128)(2,1)} %get-tuple-element.46), channel_id=1, source_target_pairs={{0,2},{2,0},{4,6},{6,4},{8,10},{10,8},{12,14},{14,12},{16,18},{18,... | collective-permute-start | bytes 3145736 | tf_op jit(solution)/shard_map/ppermute | solution.py:174
  (41 other events, 453.9 us)

commit v2 on v1

--- a/solution.py
+++ b/solution.py
@@ -368,7 +368,7 @@
 
 
 def hidden_body(gate_ref, up_ref, code_ref, around_ref, taps_ref, own_ref, other_ref):
-    each, _, rows, cells = gate_ref.shape
+    _, each, _, rows, cells = gate_ref.shape
     for b in range(each):
         out_ref = (own_ref, other_ref)[b]
         code = code_ref[b, 0].astype(full)
@@ -378,7 +378,7 @@
         for start in range(0, cells, LANES):
             size = min(LANES, cells - start)
             columns = slice(start, start + size)
-            gate = gate_ref[b, 0, :, columns].astype(full)
+            gate = gate_ref[0, b, 0, :, columns].astype(full)
             top, bottom = around_ref[b, 0, 0:1, columns], around_ref[b, 0, 1:2, columns]
             at = index[:, :size]
             before = jnp.where(at == 0, top.astype(full), pltpu.roll(gate, 1, 0))
@@ -389,7 +389,7 @@
                 + taps_ref[2:3, columns] * jnp.where(same_next[:, :size], after, 0.0)
             )
             share = 0.5 * jnp.tanh(0.5 * conv) + 0.5
-            out_ref[0, :, columns] = (conv * share * up_ref[b, 0, :, columns]).astype(low)
+            out_ref[0, :, columns] = (conv * share * up_ref[0, b, 0, :, columns]).astype(low)
 
 
 def down_body(spots, me_ref, *refs):
@@ -575,31 +575,39 @@
             hops.append((i, goal))
 
     sets = [[tokens[i] for i in (0, 2, 4, 6)], [tokens[i] for i in (1, 3, 5, 7)]]
-    made = {}
-    for c, (pieces, size) in enumerate(zip(chunks, sizes)):
-        for t, blocks in enumerate(sets):
-            made[c, t] = pl.pallas_call(
-                lambda *refs: product_body(spots(pieces), at.fars, 4, width, *refs),
-                out_shape=[
-                    jax.ShapeDtypeStruct((4, own, size), low),
-                    jax.ShapeDtypeStruct((4, own, size), full),
-                ],
-                grid=(2,),
-                in_specs=[smem()] + [hbm()] * (4 + len(pieces)),
-                out_specs=[pl.BlockSpec((2, own, size), lambda b: (b, 0, 0))] * 2,
-                scratch_shapes=[
-                    pltpu.VMEM((width, 2 * size), low),
-                    pltpu.VMEM((4 * own, width), low),
-                    pltpu.SemaphoreType.DMA((4 * len(pieces),)),
-                    pltpu.SemaphoreType.DMA((4,)),
-                ],
-                compiler_params=params,
-                cost_estimate=cost(16 * own * width * size, 8 * own * width),
-            )(me, *blocks, *[piece for _, _, piece in pieces])
+
+    def products(c, blocks):
+        pieces, size = chunks[c], sizes[c]
+        number = len(blocks)
+        gate, up = pl.pallas_call(
+            lambda *refs: product_body(spots(pieces), at.fars, number, width, *refs),
+            out_shape=[
+                jax.ShapeDtypeStruct((number, own, size), low),
+                jax.ShapeDtypeStruct((number, own, size), full),
+            ],
+            grid=(number // 2,),
+            in_specs=[smem()] + [hbm()] * (number + len(pieces)),
+            out_specs=[pl.BlockSpec((2, own, size), lambda b: (b, 0, 0))] * 2,
+            scratch_shapes=[
+                pltpu.VMEM((width, 2 * size), low),
+                pltpu.VMEM((number * own, width), low),
+                pltpu.SemaphoreType.DMA((4 * len(pieces),)),
+                pltpu.SemaphoreType.DMA((number,)),
+            ],
+            compiler_params=params,
+            cost_estimate=cost(4 * number * own * width * size, 2 * number * own * width),
+        )(me, *blocks, *[piece for _, _, piece in pieces])
+        return gate.reshape(-1, 2, 2, own, size), up.reshape(-1, 2, 2, own, size)
+
+    both = products(1, sets[0] + sets[1])
+    made = {(1, 0): (both, 0), (1, 1): (both, 1)}
+    for t in (0, 1):
+        made[0, t] = (products(0, sets[t]), 0)
 
     def ends_of(t):
-        rows_ = [jnp.concatenate([made[c, t][0][:, :1], made[c, t][0][:, -1:]], axis=1) for c in (0, 1)]
-        return jnp.concatenate(rows_, axis=2).reshape(2, 2, 2, part)
+        gates = [made[c, t][0][0][made[c, t][1]] for c in (0, 1)]
+        rows_ = [jnp.concatenate([gate[:, :, :1], gate[:, :, -1:]], axis=2) for gate in gates]
+        return jnp.concatenate(rows_, axis=3)
 
     edges = jnp.stack([ends_of(0), ends_of(1)], axis=2)
     edges = flips(edges, at).transpose(2, 1, 0, 3, 4).reshape(2, 4, 2, part)
@@ -626,13 +634,15 @@
         codes = jnp.stack([block[:, width:] for block in sets[t]]).reshape(2, 2, own, LANES)
         for c, size in enumerate(sizes):
             columns = slice(c * split, c * split + size)
+            (gate, up), place = made[c, t]
+            spec = pl.BlockSpec((1, 2, 1, own, size), lambda b, k=place: (k, 0, b, 0, 0))
             kept_hidden[c, t], sent_hidden[c, t] = pl.pallas_call(
                 hidden_body,
                 out_shape=[jax.ShapeDtypeStruct((2, own, size), low)] * 2,
                 grid=(2,),
                 in_specs=[
-                    rows_of(own, size),
-                    rows_of(own, size),
+                    spec,
+                    spec,
                     rows_of(own, LANES),
                     rows_of(2, size),
                     pl.BlockSpec((3, size), lambda b: (0, 0)),
@@ -641,8 +651,8 @@
                 compiler_params=params,
                 cost_estimate=cost(1_500_000_000, 4 * own * size * 8),
             )(
-                made[c, t][0].reshape(2, 2, own, size),
-                made[c, t][1].reshape(2, 2, own, size),
+                gate,
+                up,
                 codes,
                 around[:, :, t, :, columns],
                 taps[:, columns],

time: 285 us -> 297 us (1.042)
  waiting for transfers between devices: 111 us -> 140 us
  starting transfers between devices: 40 us -> 31.3 us
  local copies, waits for them, and re-layouts: 26.3 us -> 21.6 us
    ppermute x3, waiting for transfers between devices: 25 us -> 48.2 us  [far_shift(): return lax.ppermute(cells, 'sp', hops)]
    ppermute x20, starting transfers between devices: 28.5 us -> 21.9 us  [swap(): lax.ppermute(cells, 'sp', [(i, i ^ bit) for i in range(lax.axis_size('sp'...]
    ppermute x20, waiting for transfers between devices: 82 us -> 86.3 us  [swap(): lax.ppermute(cells, 'sp', [(i, i ^ bit) for i in range(lax.axis_size('sp'...]
    pallas_call x4 -> x3, Pallas kernels: 30.8 us -> 28.6 us  [products(): pl.pallas_call(lambda *refs: product_body(spots(pieces), at.fars, number,...]
  transfers between devices with their start and end apart: 39 -> 39, of which waited for: 15 -> 16; matrix products, arithmetic and copies ran while one was open for 11% -> 9% of each run, Pallas kernels for 28% -> 26%
where the time goes in v2:
time: 297 us; the launch traced here: 294 us
  waiting for transfers between devices  140 us (47%)
  Pallas kernels  89.6 us (30%)
  starting transfers between devices  31.3 us (11%)
  local copies, waits for them, and re-layouts  21.6 us (7%)
  other arithmetic  10.4 us (4%)
    ppermute x20, waiting for transfers between devices, swap(): lax.ppermute(cells, 'sp', [(i, i ^ bit) for i in range(lax.axis_size('sp'...  86.3 us
    ppermute x3, waiting for transfers between devices, far_shift(): return lax.ppermute(cells, 'sp', hops)  48.2 us
    pallas_call x3, Pallas kernels, products(): pl.pallas_call(lambda *refs: product_body(spots(pieces), at.fars, number,...  28.6 us
    ppermute x20, starting transfers between devices, swap(): lax.ppermute(cells, 'sp', [(i, i ^ bit) for i in range(lax.axis_size('sp'...  21.9 us
    pallas_call x2, Pallas kernels, attended(): pl.pallas_call(attend_body, out_shape=jax.ShapeDtypeStruct((own, width),...  21.6 us
    pallas_call x2, Pallas kernels, down(): pl.pallas_call(lambda *refs: down_body(picked, *refs), out_shape=[jax.Sha...  17.9 us
    pallas_call x4, Pallas kernels, local(): pl.pallas_call(hidden_body, out_shape=[jax.ShapeDtypeStruct((2, own, size...  12.7 us
    another operation x8, local copies, waits for them, and re-layouts, local(): jnp.stack([block[:, width:] for block in sets[t]]).reshape(2, 2, own, LANES)  6.01 us
  transfers between devices with their start and end apart: 39, of which 16 were waited for; matrix products, arithmetic and copies ran while one was open for 9% of the time, Pallas kernels for 26%

profile of v2, /device:TPU:0, one launch (start us, length us, event | category | flops | bytes accessed | tf_op | source)
XLA Modules:
  0.0 293.7 jit_solution(11710837131557543573)
XLA Ops:
  11.9 3.6 %collective-permute-start.15 = (bf16[2,128,768]{2,1,0:T(8,128)(2,1)}, bf16[2,128,768]{2,1,0:T(8,128)(2,1)}, u32[]{:S(2)}, u32[]{:S(2)}) collective-permute-start(bf16[2,128,768]{2,1,0:T(8,128)(2,1)} %dynamic-slice_bitcast_fusion), channel_id=1, source_target_pairs={{0,2},{2,0},{4,6},{6,4},{8,10},{10,8},{12,14},{14,12},{16,18},{18,... | collective-permute-start | bytes 1179656 | tf_op jit(solution)/shard_map/ppermute | solution.py:174
  18.6 3.4 %collective-permute-done = bf16[128,640]{1,0:T(8,128)(2,1)S(1)} collective-permute-done((bf16[128,640]{1,0:T(8,128)(2,1)}, bf16[128,640]{1,0:T(8,128)(2,1)S(1)}, u32[]{:S(2)}, u32[]{:S(2)}) %collective-permute-start) | collective-permute-done | bytes 163872 | tf_op jit(solution)/shard_map/ppermute | solution.py:513
  24.4 10.9 %shard_map.119 = bf16[256,2048]{1,0:T(8,128)(2,1)} custom-call(s32[1]{0:T(128)S(6)} %sub.9.half_ref, f32[16]{0:T(128)} %sink_ref.3, bf16[512,1024]{1,0:T(8,128)(2,1)} %q_ref.3, bf16[768,640]{1,0:T(8,128)(2,1)} %pad_maximum_fusion.near_ref, f32[768,128]{1,0:T(8,128)} %get-tuple-element.100.cos_ref, f32[768,128]{1,0:T(8,128)} %get-tuple-element.101.sin_ref, ...), custom_call_target="tpu_custom_call" | custom-call | flops 8999999488 | bytes 6000000 | tf_op jit(solution)/shard_map/pallas_call | solution.py:531
  38.4 10.7 %shard_map.118.own_ref = bf16[256,2048]{1,0:T(8,128)(2,1)} custom-call(s32[1]{0:T(128)} %bitcast.1.half_ref.core_ref, f32[16]{0:T(128)} %sink_ref.3, bf16[512,1024]{1,0:T(8,128)(2,1)} %q_ref.3, bf16[768,640]{1,0:T(8,128)(2,1)} %pad_maximum_fusion.near_ref, f32[768,128]{1,0:T(8,128)} %get-tuple-element.100.cos_ref, f32[768,128]{1,0:T(8,128)} %get-tuple-element.101.sin_ref, ...), custom_call_target="tpu_custom_call" | custom-call | flops 8999999488 | bytes 6000000 | tf_op jit(solution)/shard_map/pallas_call | solution.py:531
  49.2 4.3 %norm.1 = (bf16[256,2048]{1,0:T(8,128)(2,1)}, bf16[256,2176]{1,0:T(8,128)(2,1)}) custom-call(s32[1]{0:T(128)} %bitcast.1.half_ref.core_ref, bf16[256,2048]{1,0:T(8,128)(2,1)} %residual_ref.1, bf16[256,2048]{1,0:T(8,128)(2,1)} %shard_map.118.own_ref, bf16[256,2048]{1,0:T(8,128)(2,1)} %collective-permute-done.2.given_ref, f32[3,2048]{1,0:T(4,128)} %gains_ref.1, ...), custom_call_target="tpu_custom_call" | custom-call | flops 2000000000 | bytes 6291456 | tf_op jit(solution)/shard_map/norm/pallas_call | solution.py:550
  59.6 29.9 %collective-permute-done.16 = bf16[2,128,768]{2,1,0:T(8,128)(2,1)S(1)} collective-permute-done((bf16[2,128,768]{2,1,0:T(8,128)(2,1)S(1)}, bf16[2,128,768]{2,1,0:T(8,128)(2,1)S(1)}, u32[]{:S(2)}, u32[]{:S(2)}) %collective-permute-start.16) | collective-permute-done | bytes 393248 | tf_op jit(solution)/shard_map/ppermute | solution.py:174
  92.3 9.6 %collective-permute-done.25 = bf16[2,128,640]{2,1,0:T(8,128)(2,1)S(1)} collective-permute-done((bf16[2,128,640]{2,1,0:T(8,128)(2,1)S(1)}, bf16[2,128,640]{2,1,0:T(8,128)(2,1)S(1)}, u32[]{:S(2)}, u32[]{:S(2)}) %collective-permute-start.25) | collective-permute-done | bytes 327712 | tf_op jit(solution)/shard_map/ppermute | solution.py:174
  103.4 16.1 %collective-permute-done.4 = bf16[2,704,128]{2,1,0:T(8,128)(2,1)S(1)} collective-permute-done((bf16[2,704,128]{2,1,0:T(8,128)(2,1)S(1)}, bf16[2,704,128]{2,1,0:T(8,128)(2,1)S(1)}, u32[]{:S(2)}, u32[]{:S(2)}) %collective-permute-start.4) | collective-permute-done | bytes 360480 | tf_op jit(solution)/shard_map/ppermute | solution.py:174
  120.6 5.0 %collective-permute-done.18.refs_7_ = bf16[4,128,768]{2,1,0:T(8,128)(2,1)} collective-permute-done((bf16[4,128,768]{2,1,0:T(8,128)(2,1)S(1)}, bf16[4,128,768]{2,1,0:T(8,128)(2,1)}, u32[]{:S(2)}, u32[]{:S(2)}) %collective-permute-start.18) | collective-permute-done | bytes 786464 | tf_op jit(solution)/shard_map/ppermute | solution.py:197
  129.6 27.0 %collective-permute-done.27.refs_11_ = bf16[4,128,640]{2,1,0:T(8,128)(2,1)} collective-permute-done((bf16[4,128,640]{2,1,0:T(8,128)(2,1)S(1)}, bf16[4,128,640]{2,1,0:T(8,128)(2,1)}, u32[]{:S(2)}, u32[]{:S(2)}) %collective-permute-start.27) | collective-permute-done | bytes 655392 | tf_op jit(solution)/shard_map/ppermute | solution.py:197
  158.7 7.7 %shard_map.120 = (bf16[4,256,384]{2,1,0:T(8,128)(2,1)}, f32[4,256,384]{2,1,0:T(8,128)}) custom-call(s32[1]{0:T(128)} %bitcast.refs_0_, bf16[256,2176]{1,0:T(8,128)(2,1)} %get-tuple-element.26.refs_1_, bf16[256,2176]{1,0:T(8,128)(2,1)} %collective-permute-done.12.refs_2_, bf16[256,2176]{1,0:T(8,128)(2,1)} %collective-permute-done.13.refs_3_, ...), custom_call_target="tpu_custom_call" | custom-call | flops 3221225472 | bytes 4194304 | tf_op jit(solution)/shard_map/pallas_call | solution.py:582
  170.8 3.4 %collective-permute-done.26.refs_10_ = bf16[4,128,640]{2,1,0:T(8,128)(2,1)} collective-permute-done((bf16[4,128,640]{2,1,0:T(8,128)(2,1)S(1)}, bf16[4,128,640]{2,1,0:T(8,128)(2,1)}, u32[]{:S(2)}, u32[]{:S(2)}) %collective-permute-start.26) | collective-permute-done | bytes 655392 | tf_op jit(solution)/shard_map/ppermute | solution.py:174
  174.2 16.2 %collective-permute-done.6.refs_3_ = bf16[4,704,128]{2,1,0:T(8,128)(2,1)S(1)} collective-permute-done((bf16[4,704,128]{2,1,0:T(8,128)(2,1)S(1)}, bf16[4,704,128]{2,1,0:T(8,128)(2,1)S(1)}, u32[]{:S(2)}, u32[]{:S(2)}) %collective-permute-start.6) | collective-permute-done | bytes 720928 | tf_op jit(solution)/shard_map/ppermute | solution.py:197
  192.0 12.9 %shard_map.121 = (bf16[8,256,320]{2,1,0:T(8,128)(2,1)}, f32[8,256,320]{2,1,0:T(8,128)}) custom-call(s32[1]{0:T(128)} %bitcast.refs_0_, bf16[256,2176]{1,0:T(8,128)(2,1)} %get-tuple-element.26.refs_1_, bf16[256,2176]{1,0:T(8,128)(2,1)} %collective-permute-done.12.refs_2_, bf16[256,2176]{1,0:T(8,128)(2,1)} %collective-permute-done.13.refs_3_, ...), custom_call_target="tpu_custom_call" | custom-call | flops 5368709120 | bytes 8388608 | tf_op jit(solution)/shard_map/pallas_call | solution.py:582
  206.5 8.0 %shard_map.122 = (bf16[4,256,384]{2,1,0:T(8,128)(2,1)}, f32[4,256,384]{2,1,0:T(8,128)}) custom-call(s32[1]{0:T(128)} %bitcast.refs_0_, bf16[256,2176]{1,0:T(8,128)(2,1)} %collective-permute-done.20.refs_5_.refs_1_, bf16[256,2176]{1,0:T(8,128)(2,1)} %collective-permute-done.21.refs_6_.refs_2_, bf16[256,2176]{1,0:T(8,128)(2,1)} %collective-permute-done.22.refs_7_.refs_3_, ...), custom_call_target="tpu_custom_call" | custom-call | flops 3221225472 | bytes 4194304 | tf_op jit(solution)/shard_map/pallas_call | solution.py:582
  220.2 3.2 %shard_map.125 = (bf16[2,256,384]{2,1,0:T(8,128)(2,1)}, bf16[2,256,384]{2,1,0:T(8,128)(2,1)}) custom-call(bf16[1,2,2,256,384]{4,3,2,1,0:T(8,128)(2,1)} %bitcast.139, f32[1,2,2,256,384]{4,3,2,1,0:T(8,128)} %bitcast.143, bf16[2,2,256,128]{3,2,1,0:T(8,128)(2,1)} %bitcast.123, bf16[2,2,2,384]{3,2,1,0:T(2,128)(2,1)} %get-tuple-element.87.around_ref, ...), custom_call_target="tpu_custom_call" | custom-call | flops 1500000000 | bytes 3145728 | tf_op jit(solution)/shard_map/pallas_call | solution.py:639
  224.3 3.1 %shard_map.126 = (bf16[2,256,320]{2,1,0:T(8,128)(2,1)}, bf16[2,256,320]{2,1,0:T(8,128)(2,1)}) custom-call(bf16[2,2,2,256,320]{4,3,2,1,0:T(8,128)(2,1)} %bitcast.115, f32[2,2,2,256,320]{4,3,2,1,0:T(8,128)} %bitcast.140, bf16[2,2,256,128]{3,2,1,0:T(8,128)(2,1)} %bitcast.124, bf16[2,2,2,320]{3,2,1,0:T(2,128)(2,1)} %get-tuple-element.85.around_ref, ...), custom_call_target="tpu_custom_call" | custom-call | flops 1500000000 | bytes 2621440 | tf_op jit(solution)/shard_map/pallas_call | solution.py:639
  227.5 3.2 %shard_map.123 = (bf16[2,256,384]{2,1,0:T(8,128)(2,1)}, bf16[2,256,384]{2,1,0:T(8,128)(2,1)}) custom-call(bf16[1,2,2,256,384]{4,3,2,1,0:T(8,128)(2,1)} %bitcast.137, f32[1,2,2,256,384]{4,3,2,1,0:T(8,128)} %bitcast.142, bf16[2,2,256,128]{3,2,1,0:T(8,128)(2,1)} %bitcast.121, bf16[2,2,2,384]{3,2,1,0:T(2,128)(2,1)} %get-tuple-element.88.around_ref, ...), custom_call_target="tpu_custom_call" | custom-call | flops 1500000000 | bytes 3145728 | tf_op jit(solution)/shard_map/pallas_call | solution.py:639
  230.9 3.2 %shard_map.124 = (bf16[2,256,320]{2,1,0:T(8,128)(2,1)}, bf16[2,256,320]{2,1,0:T(8,128)(2,1)}) custom-call(bf16[2,2,2,256,320]{4,3,2,1,0:T(8,128)(2,1)} %bitcast.116, f32[2,2,2,256,320]{4,3,2,1,0:T(8,128)} %bitcast.141, bf16[2,2,256,128]{3,2,1,0:T(8,128)(2,1)} %bitcast.122, bf16[2,2,2,320]{3,2,1,0:T(2,128)(2,1)} %get-tuple-element.86.around_ref, ...), custom_call_target="tpu_custom_call" | custom-call | flops 1500000000 | bytes 2621440 | tf_op jit(solution)/shard_map/pallas_call | solution.py:639
  237.6 9.0 %shard_map.128 = (bf16[2,256,1024]{2,1,0:T(8,128)(2,1)}, bf16[2,256,1024]{2,1,0:T(8,128)(2,1)}) custom-call(s32[1]{0:T(128)} %bitcast.refs_0_, bf16[4,704,128]{2,1,0:T(8,128)(2,1)} %copy-done.9, bf16[4,704,128]{2,1,0:T(8,128)(2,1)} %collective-permute-done.5.refs_2_, bf16[4,704,128]{2,1,0:T(8,128)(2,1)} %copy-done.17, ...), custom_call_target="tpu_custom_call" | custom-call | flops 2952790016 | bytes 3145728 | tf_op jit(solution)/shard_map/pallas_call | solution.py:670
  247.8 8.9 %shard_map.127 = (bf16[2,256,1024]{2,1,0:T(8,128)(2,1)}, bf16[2,256,1024]{2,1,0:T(8,128)(2,1)}) custom-call(s32[1]{0:T(128)} %bitcast.refs_0_, bf16[4,704,128]{2,1,0:T(8,128)(2,1)} %copy-done.9, bf16[4,704,128]{2,1,0:T(8,128)(2,1)} %collective-permute-done.5.refs_2_, bf16[4,704,128]{2,1,0:T(8,128)(2,1)} %copy-done.17, ...), custom_call_target="tpu_custom_call" | custom-call | flops 2952790016 | bytes 3145728 | tf_op jit(solution)/shard_map/pallas_call | solution.py:670
  256.8 15.4 %collective-permute-done.37.refs_7_ = bf16[2,256,1024]{2,1,0:T(8,128)(2,1)S(1)} collective-permute-done((bf16[2,256,1024]{2,1,0:T(8,128)(2,1)}, bf16[2,256,1024]{2,1,0:T(8,128)(2,1)S(1)}, u32[]{:S(2)}, u32[]{:S(2)}) %collective-permute-start.37) | collective-permute-done | bytes 1048608 | tf_op jit(solution)/shard_map/ppermute | solution.py:174
  277.0 10.2 %collective-permute-done.38.refs_8_ = bf16[256,1024]{1,0:T(8,128)(2,1)S(1)} collective-permute-done((bf16[256,1024]{1,0:T(8,128)(2,1)S(1)}, bf16[256,1024]{1,0:T(8,128)(2,1)S(1)}, u32[]{:S(2)}, u32[]{:S(2)}) %collective-permute-start.38) | collective-permute-done | bytes 524320 | tf_op jit(solution)/shard_map/ppermute | solution.py:174
  289.2 4.5 %final.1 = bf16[256,2048]{1,0:T(8,128)(2,1)} custom-call(s32[1]{0:T(128)} %bitcast.refs_0_, bf16[256,2048]{1,0:T(8,128)(2,1)} %get-tuple-element.25.refs_1_, f32[1,2048]{1,0:T(1,128)} %slice.181.refs_2_, bf16[2,256,1024]{2,1,0:T(8,128)(2,1)} %get-tuple-element.41.refs_3_, bf16[2,256,1024]{2,1,0:T(8,128)(2,1)} %copy-done.1, bf16[256,1024]{1,0:T(8,128)(2,1)} %copy-done.12, ...), custom_call_target="tpu_custom_call" | custom-call | flops 5242880 | bytes 7340032 | tf_op jit(solution)/shard_map/final/pallas_call | solution.py:699
  (201 shorter events, 63.5 us)
Async XLA Ops:
  3.6 53.2 %collective-permute-start.24 = (bf16[2,128,640]{2,1,0:T(8,128)(2,1)}, bf16[2,128,640]{2,1,0:T(8,128)(2,1)}, u32[]{:S(2)}, u32[]{:S(2)}) collective-permute-start(bf16[2,128,640]{2,1,0:T(8,128)(2,1)} %dynamic-slice_bitcast_fusion.2), channel_id=1, source_target_pairs={{0,2},{2,0},{4,6},{6,4},{8,10},{10,8},{12,14},{14,12},{16,18},{18,... | collective-permute-start | bytes 983048 | tf_op jit(solution)/shard_map/ppermute | solution.py:174
  11.9 43.2 %collective-permute-start.15 = (bf16[2,128,768]{2,1,0:T(8,128)(2,1)}, bf16[2,128,768]{2,1,0:T(8,128)(2,1)}, u32[]{:S(2)}, u32[]{:S(2)}) collective-permute-start(bf16[2,128,768]{2,1,0:T(8,128)(2,1)} %dynamic-slice_bitcast_fusion), channel_id=1, source_target_pairs={{0,2},{2,0},{4,6},{6,4},{8,10},{10,8},{12,14},{14,12},{16,18},{18,... | collective-permute-start | bytes 1179656 | tf_op jit(solution)/shard_map/ppermute | solution.py:174
  35.4 24.2 %collective-permute-start.3 = (bf16[2,704,128]{2,1,0:T(8,128)(2,1)S(1)}, bf16[2,704,128]{2,1,0:T(8,128)(2,1)S(1)}, u32[]{:S(2)}, u32[]{:S(2)}) collective-permute-start(bf16[2,704,128]{2,1,0:T(8,128)(2,1)S(1)} %dynamic-slice_bitcast_fusion.1), channel_id=1, source_target_pairs={{0,2},{2,0},{4,6},{6,4},{8,10},{10,8},{12,14},{14,12},{16,18},{18,... | collective-permute-start | bytes 1081352 | tf_op jit(solution)/shard_map/ppermute | solution.py:174
  53.4 48.4 %collective-permute-start.20 = (bf16[256,2176]{1,0:T(8,128)(2,1)}, bf16[256,2176]{1,0:T(8,128)(2,1)}, u32[]{:S(2)}, u32[]{:S(2)}) collective-permute-start(bf16[256,2176]{1,0:T(8,128)(2,1)} %get-tuple-element.26.refs_1_), channel_id=1, source_target_pairs={{0,8},{2,10},{4,12},{6,14},{8,0},{10,2},{12,4},{14,6},{16,24},{18,... | collective-permute-start | bytes 3342344 | tf_op jit(solution)/shard_map/ppermute | solution.py:174
  55.0 48.2 %collective-permute-start.12 = (bf16[256,2176]{1,0:T(8,128)(2,1)}, bf16[256,2176]{1,0:T(8,128)(2,1)}, u32[]{:S(2)}, u32[]{:S(2)}) collective-permute-start(bf16[256,2176]{1,0:T(8,128)(2,1)} %get-tuple-element.26.refs_1_), channel_id=1, source_target_pairs={{0,2},{2,0},{4,6},{6,4},{8,10},{10,8},{12,14},{14,12},{16,18},{18,... | collective-permute-start | bytes 3342344 | tf_op jit(solution)/shard_map/ppermute | solution.py:174
  56.2 33.3 %collective-permute-start.16 = (bf16[2,128,768]{2,1,0:T(8,128)(2,1)S(1)}, bf16[2,128,768]{2,1,0:T(8,128)(2,1)S(1)}, u32[]{:S(2)}, u32[]{:S(2)}) collective-permute-start(bf16[2,128,768]{2,1,0:T(8,128)(2,1)S(1)} %pad_maximum_fusion.8), channel_id=1, source_target_pairs={{0,8},{2,10},{4,12},{6,14},{8,0},{10,2},{12,4},{14,6},{16,24},{18,... | collective-permute-start | bytes 1179656 | tf_op jit(solution)/shard_map/ppermute | solution.py:174
  57.9 44.0 %collective-permute-start.25 = (bf16[2,128,640]{2,1,0:T(8,128)(2,1)S(1)}, bf16[2,128,640]{2,1,0:T(8,128)(2,1)S(1)}, u32[]{:S(2)}, u32[]{:S(2)}) collective-permute-start(bf16[2,128,640]{2,1,0:T(8,128)(2,1)S(1)} %pad_maximum_fusion.10), channel_id=1, source_target_pairs={{0,8},{2,10},{4,12},{6,14},{8,0},{10,2},{12,4},{14,6},{16,24},{18,... | collective-permute-start | bytes 983048 | tf_op jit(solution)/shard_map/ppermute | solution.py:174
  59.6 66.9 %collective-permute-start.13 = (bf16[256,2176]{1,0:T(8,128)(2,1)}, bf16[256,2176]{1,0:T(8,128)(2,1)}, u32[]{:S(2)}, u32[]{:S(2)}) collective-permute-start(bf16[256,2176]{1,0:T(8,128)(2,1)} %get-tuple-element.26.refs_1_), channel_id=1, source_target_pairs={{0,1},{1,0},{2,3},{3,2},{4,5},{5,4},{6,7},{7,6},{8,9},{9,8},{10,11... | collective-permute-start | bytes 3342344 | tf_op jit(solution)/shard_map/ppermute | solution.py:193
  89.6 36.0 %collective-permute-start.18 = (bf16[4,128,768]{2,1,0:T(8,128)(2,1)S(1)}, bf16[4,128,768]{2,1,0:T(8,128)(2,1)}, u32[]{:S(2)}, u32[]{:S(2)}) collective-permute-start(bf16[4,128,768]{2,1,0:T(8,128)(2,1)S(1)} %pad_maximum_fusion.2.refs_5_), channel_id=1, source_target_pairs={{0,16},{2,18},{4,20},{6,22},{8,24},{10,26},{12,28},{14,30},{16,0},... | collective-permute-start | bytes 2359304 | tf_op jit(solution)/shard_map/ppermute | solution.py:197
  101.9 26.2 %collective-permute-start.21 = (bf16[256,2176]{1,0:T(8,128)(2,1)}, bf16[256,2176]{1,0:T(8,128)(2,1)}, u32[]{:S(2)}, u32[]{:S(2)}) collective-permute-start(bf16[256,2176]{1,0:T(8,128)(2,1)} %collective-permute-done.20.refs_5_.refs_1_), channel_id=1, source_target_pairs={{0,2},{2,0},{4,6},{6,4},{8,10},{10,8},{12,14},{14,12},{16,18},{18,... | collective-permute-start | bytes 3342344 | tf_op jit(solution)/shard_map/ppermute | solution.py:174
  103.3 25.7 %collective-permute-start.14 = (bf16[256,2176]{1,0:T(8,128)(2,1)}, bf16[256,2176]{1,0:T(8,128)(2,1)S(1)}, u32[]{:S(2)}, u32[]{:S(2)}) collective-permute-start(bf16[256,2176]{1,0:T(8,128)(2,1)} %collective-permute-done.12.refs_2_), channel_id=1, source_target_pairs={{0,1},{1,0},{2,3},{3,2},{4,5},{5,4},{6,7},{7,6},{8,9},{9,8},{10,11... | collective-permute-start | bytes 3342344 | tf_op jit(solution)/shard_map/ppermute | solution.py:193
  119.6 38.1 %collective-permute-start.17 = (bf16[4,128,768]{2,1,0:T(8,128)(2,1)S(1)}, bf16[4,128,768]{2,1,0:T(8,128)(2,1)S(1)}, u32[]{:S(2)}, u32[]{:S(2)}) collective-permute-start(bf16[4,128,768]{2,1,0:T(8,128)(2,1)S(1)} %pad_maximum_fusion.2.refs_5_), channel_id=1, source_target_pairs={{0,4},{2,6},{4,0},{6,2},{8,12},{10,14},{12,8},{14,10},{16,20},{18,... | collective-permute-start | bytes 2359304 | tf_op jit(solution)/shard_map/ppermute | solution.py:174
  125.6 32.2 %collective-permute-start.19 = (bf16[4,128,768]{2,1,0:T(8,128)(2,1)}, bf16[4,128,768]{2,1,0:T(8,128)(2,1)}, u32[]{:S(2)}, u32[]{:S(2)}) collective-permute-start(bf16[4,128,768]{2,1,0:T(8,128)(2,1)} %collective-permute-done.18.refs_7_), channel_id=1, source_target_pairs={{0,4},{2,6},{4,0},{6,2},{8,12},{10,14},{12,8},{14,10},{16,20},{18,... | collective-permute-start | bytes 2359304 | tf_op jit(solution)/shard_map/ppermute | solution.py:174
  126.5 30.0 %collective-permute-start.27 = (bf16[4,128,640]{2,1,0:T(8,128)(2,1)S(1)}, bf16[4,128,640]{2,1,0:T(8,128)(2,1)}, u32[]{:S(2)}, u32[]{:S(2)}) collective-permute-start(bf16[4,128,640]{2,1,0:T(8,128)(2,1)S(1)} %pad_maximum_fusion.5.refs_9_), channel_id=1, source_target_pairs={{0,16},{2,18},{4,20},{6,22},{8,24},{10,26},{12,28},{14,30},{16,0},... | collective-permute-start | bytes 1966088 | tf_op jit(solution)/shard_map/ppermute | solution.py:197
  128.1 40.7 %collective-permute-start.22 = (bf16[256,2176]{1,0:T(8,128)(2,1)}, bf16[256,2176]{1,0:T(8,128)(2,1)}, u32[]{:S(2)}, u32[]{:S(2)}) collective-permute-start(bf16[256,2176]{1,0:T(8,128)(2,1)} %collective-permute-done.20.refs_5_.refs_1_), channel_id=1, source_target_pairs={{0,1},{1,0},{2,3},{3,2},{4,5},{5,4},{6,7},{7,6},{8,9},{9,8},{10,11... | collective-permute-start | bytes 3342344 | tf_op jit(solution)/shard_map/ppermute | solution.py:193
  129.0 63.0 %collective-permute-start.23 = (bf16[256,2176]{1,0:T(8,128)(2,1)}, bf16[256,2176]{1,0:T(8,128)(2,1)}, u32[]{:S(2)}, u32[]{:S(2)}) collective-permute-start(bf16[256,2176]{1,0:T(8,128)(2,1)} %collective-permute-done.21.refs_6_.refs_2_), channel_id=1, source_target_pairs={{0,1},{1,0},{2,3},{3,2},{4,5},{5,4},{6,7},{7,6},{8,9},{9,8},{10,11... | collective-permute-start | bytes 3342344 | tf_op jit(solution)/shard_map/ppermute | solution.py:193
  156.5 17.7 %collective-permute-start.26 = (bf16[4,128,640]{2,1,0:T(8,128)(2,1)S(1)}, bf16[4,128,640]{2,1,0:T(8,128)(2,1)}, u32[]{:S(2)}, u32[]{:S(2)}) collective-permute-start(bf16[4,128,640]{2,1,0:T(8,128)(2,1)S(1)} %pad_maximum_fusion.5.refs_9_), channel_id=1, source_target_pairs={{0,4},{2,6},{4,0},{6,2},{8,12},{10,14},{12,8},{14,10},{16,20},{18,... | collective-permute-start | bytes 1966088 | tf_op jit(solution)/shard_map/ppermute | solution.py:174
  157.7 32.7 %collective-permute-start.6 = (bf16[4,704,128]{2,1,0:T(8,128)(2,1)S(1)}, bf16[4,704,128]{2,1,0:T(8,128)(2,1)S(1)}, u32[]{:S(2)}, u32[]{:S(2)}) collective-permute-start(bf16[4,704,128]{2,1,0:T(8,128)(2,1)S(1)} %pad_maximum_fusion.3.refs_1_), channel_id=1, source_target_pairs={{0,16},{2,18},{4,20},{6,22},{8,24},{10,26},{12,28},{14,30},{16,0},... | collective-permute-start | bytes 2162696 | tf_op jit(solution)/shard_map/ppermute | solution.py:197
  157.8 34.2 %collective-permute-start.28 = (bf16[4,128,640]{2,1,0:T(8,128)(2,1)}, bf16[4,128,640]{2,1,0:T(8,128)(2,1)}, u32[]{:S(2)}, u32[]{:S(2)}) collective-permute-start(bf16[4,128,640]{2,1,0:T(8,128)(2,1)} %collective-permute-done.27.refs_11_), channel_id=1, source_target_pairs={{0,4},{2,6},{4,0},{6,2},{8,12},{10,14},{12,8},{14,10},{16,20},{18,... | collective-permute-start | bytes 1966088 | tf_op jit(solution)/shard_map/ppermute | solution.py:174
  168.8 49.7 %collective-permute-start.5 = (bf16[4,704,128]{2,1,0:T(8,128)(2,1)S(1)}, bf16[4,704,128]{2,1,0:T(8,128)(2,1)}, u32[]{:S(2)}, u32[]{:S(2)}) collective-permute-start(bf16[4,704,128]{2,1,0:T(8,128)(2,1)S(1)} %pad_maximum_fusion.3.refs_1_), channel_id=1, source_target_pairs={{0,4},{2,6},{4,0},{6,2},{8,12},{10,14},{12,8},{14,10},{16,20},{18,... | collective-permute-start | bytes 2162696 | tf_op jit(solution)/shard_map/ppermute | solution.py:174
  174.2 56.4 %collective-permute-start.8 = (bf16[4,704,128]{2,1,0:T(8,128)(2,1)S(1)}, bf16[4,704,128]{2,1,0:T(8,128)(2,1)S(1)}, u32[]{:S(2)}, u32[]{:S(2)}) collective-permute-start(bf16[4,704,128]{2,1,0:T(8,128)(2,1)S(1)} %pad_maximum_fusion.3.refs_1_), channel_id=1, source_target_pairs={{0,1},{1,0},{2,3},{3,2},{4,5},{5,4},{6,7},{7,6},{8,9},{9,8},{10,11... | collective-permute-start | bytes 2162696 | tf_op jit(solution)/shard_map/ppermute | solution.py:193
  190.4 28.2 %collective-permute-start.7 = (bf16[4,704,128]{2,1,0:T(8,128)(2,1)S(1)}, bf16[4,704,128]{2,1,0:T(8,128)(2,1)}, u32[]{:S(2)}, u32[]{:S(2)}) collective-permute-start(bf16[4,704,128]{2,1,0:T(8,128)(2,1)S(1)} %collective-permute-done.6.refs_3_), channel_id=1, source_target_pairs={{0,4},{2,6},{4,0},{6,2},{8,12},{10,14},{12,8},{14,10},{16,20},{18,... | collective-permute-start | bytes 2162696 | tf_op jit(solution)/shard_map/ppermute | solution.py:174
  246.5 25.7 %collective-permute-start.37 = (bf16[2,256,1024]{2,1,0:T(8,128)(2,1)}, bf16[2,256,1024]{2,1,0:T(8,128)(2,1)S(1)}, u32[]{:S(2)}, u32[]{:S(2)}) collective-permute-start(bf16[2,256,1024]{2,1,0:T(8,128)(2,1)} %get-tuple-element.44), channel_id=1, source_target_pairs={{0,8},{2,10},{4,12},{6,14},{8,0},{10,2},{12,4},{14,6},{16,24},{18,... | collective-permute-start | bytes 3145736 | tf_op jit(solution)/shard_map/ppermute | solution.py:174
  246.6 28.5 %collective-permute-start.35 = (bf16[2,256,1024]{2,1,0:T(8,128)(2,1)}, bf16[2,256,1024]{2,1,0:T(8,128)(2,1)S(1)}, u32[]{:S(2)}, u32[]{:S(2)}) collective-permute-start(bf16[2,256,1024]{2,1,0:T(8,128)(2,1)} %get-tuple-element.42), channel_id=1, source_target_pairs={{0,2},{2,0},{4,6},{6,4},{8,10},{10,8},{12,14},{14,12},{16,18},{18,... | collective-permute-start | bytes 3145736 | tf_op jit(solution)/shard_map/ppermute | solution.py:174
  (40 other events, 467.1 us)
